TPU v7x, 32 devices: a whole 2x2x4 slice. The times are simulated.
32 devices in a mesh: ep: 8 (over z, y), tp: 4 (over x, core).
Axes of the slice: x: 2, y: 2, z: 4, core: 2. Of those that a mesh axis runs over, the one named last changes fastest.
Arguments:
- mixer_in: bfloat16 [4096, 2048], P('ep'), may hold values from -6 to 6
- mixer_gain: float32 [2048], replicated, may hold values from 0.1 to 1.9
- query_weight: bfloat16 [2048, 1024], P(None, 'tp'), may hold values from -0.125 to 0.125
- key_weight: bfloat16 [2048, 1024], P(None, 'tp'), may hold values from -0.125 to 0.125
- value_weight: bfloat16 [2048, 1024], P(None, 'tp'), may hold values from -0.125 to 0.125
- input_gate: float32 [8, 4096], P('tp', 'ep'), may hold values from -4 to 240
- forget_gate: float32 [8, 4096], P('tp', 'ep'), may hold values from 0 to 25
- head_gain: float32 [1024], replicated, may hold values from 0.1 to 1.9
- mixer_out_weight: bfloat16 [1024, 2048], P('tp'), may hold values from -0.1875 to 0.1875
- expert_in: bfloat16 [2048, 2048], P('ep'), may hold values from -6 to 6
- expert_gain: float32 [2048], replicated, may hold values from 0.1 to 1.9
- group_router: bfloat16 [2048, 2], replicated, may hold values from -0.125 to 0.125
- expert_router: bfloat16 [2048, 8], replicated, may hold values from -0.125 to 0.125
- routes: int32 [2048, 2], P('ep'), may hold values from 0 to 7, all different within a row; in each aligned block of 256 rows (0 to 255, 256 to 511, ...) at most 128 rows name the same one
- gate_experts: bfloat16 [8, 2048, 1024], P('ep', None, 'tp'), may hold values from -0.125 to 0.125
- up_experts: bfloat16 [8, 2048, 1024], P('ep', None, 'tp'), may hold values from -0.125 to 0.125
- down_experts: bfloat16 [8, 1024, 2048], P('ep', 'tp'), may hold values from -0.1875 to 0.1875
Outputs:
- mixer_out: bfloat16 [4096, 2048], P(('ep', 'tp'))
- expert_out: bfloat16 [2048, 2048], P('ep', 'tp')
Inputs may be any that keep to these rules, and one draw needn't show every extreme that they name: `routes`: each row names 2 different experts. In each aligned block of 256 rows (the rows of one index of ep) no expert is named by more than 128 rows, a bound that some block reaches.
All inputs are finite; a program needn't handle non-finite values.
Results may differ from a plain program's by a relative error of at most 0.014.
The roundings to bfloat16 on the way count: a program that leaves them out, or rounds other values in their place, can miss the bound.
Values may be sent and summed in bfloat16 or wider, within the bound.
A program may use at most 128 MiB of HBM per device.

v0:
```python
import functools

import jax
import jax.numpy as jnp
from jax import lax
from jax.experimental import pallas as pl
from jax.experimental.pallas import tpu as pltpu
from jax.sharding import PartitionSpec as P

MESH = pl.DeviceIdType.MESH


epsilon = 1e-06
highest = lax.Precision.HIGHEST
floor_log = -1e30


def rms_rows(matrix, gain):
    widened = matrix.astype(jnp.float32)
    scaled = widened * lax.rsqrt(jnp.mean(widened * widened, axis=-1, keepdims=True) + epsilon)
    return scaled * gain


def expert_kernel(
    sizes, own_ref, gate_ref, up_ref, down_ref, mix_ref,
    packed_ref, query_ref, key_ref, value_ref, cum_ref, cum_col_ref, in_ref, gain_ref, project_ref,
    out_ref, mixed_ref,
    rows, part, pin, csum, xin, fin, ret,
    mem, state, state_peak, state_parts, mpart, mpin, msum, mxin,
    own_sem, send_a, recv_a, send_x, recv_x, send_p, recv_p,
    send_q, recv_q, send_c, recv_c, send_r, recv_r,
    send_m, recv_m, send_h, recv_h, send_y, recv_y,
):
    n, share, cap, width, quarter = sizes
    me, tp = lax.axis_index("ep"), lax.axis_index("tp")
    pair = tp + 1 - 2 * lax.rem(tp, 2)
    cross = lax.rem(tp + 2, 4)
    pair_cross = lax.rem(pair + 2, 4)

    def remote(src, dst, send, recv, to):
        return pltpu.make_async_remote_copy(
            src_ref=src, dst_ref=dst, send_sem=send, recv_sem=recv, device_id=to, device_id_type=MESH
        )

    barrier = pltpu.get_barrier_semaphore()
    for i in range(1, n):
        pl.semaphore_signal(
            barrier, inc=1, device_id=(lax.rem(me + i, n), tp), device_id_type=MESH
        )
    pl.semaphore_signal(barrier, inc=1, device_id=(me, pair), device_id_type=MESH)
    pl.semaphore_signal(barrier, inc=1, device_id=(me, cross), device_id_type=MESH)
    own = pltpu.make_async_copy(own_ref.at[me], rows.at[me, tp], own_sem)
    own.start()
    pl.semaphore_wait(barrier, n + 1)

    def scatter(i, place):
        to = lax.rem(me + i, n)
        return remote(own_ref.at[to], rows.at[place, tp], send_a.at[i], recv_a.at[i], (to, tp))

    def across(s):
        return remote(rows.at[s, tp], rows.at[s, tp], send_x.at[s], recv_x.at[s], (me, cross))

    def beside(s, k, who):
        return remote(
            rows.at[s, who], rows.at[s, who], send_p.at[s, k], recv_p.at[s, k], (me, pair)
        )

    def halves(s, k, who):
        return remote(part.at[s, who], pin.at[s, k], send_q.at[s, k], recv_q.at[s, k], (me, pair))

    def summed(s):
        return remote(csum.at[s], xin.at[s], send_c.at[s], recv_c.at[s], (me, cross))

    def back(i):
        to = lax.rem(me + n - i, n)
        return remote(fin.at[to], ret.at[me], send_r.at[i], recv_r.at[i], (to, tp))

    def memory(i):
        return remote(
            packed_ref, mem.at[i], send_m.at[i], recv_m.at[i], (lax.rem(me + i, n), tp)
        )

    def mixed_half(k, who):
        return remote(mpart.at[who], mpin.at[k], send_h.at[k], recv_h.at[k], (me, pair))

    def mixed_sum():
        return remote(msum, mxin, send_y, recv_y, (me, cross))

    def first(i, carry):
        scatter(i, me).start()
        return carry

    def second(i, carry):
        @pl.when(me + i < n)
        def _():
            memory(i).start()

        return carry

    heads = packed_ref.shape[0]
    size = packed_ref.shape[2]
    length = query_ref.shape[0]
    chunk = length // 4
    scale = size ** (-0.5)

    def prefix():
        state[...] = jnp.zeros_like(state)
        state_peak[...] = jnp.full_like(state_peak, floor_log)

        def merge(k, carry):
            i = n - 1 - k

            @pl.when(i <= me)
            def _():
                memory(i).wait_recv()
                for h in range(heads):
                    later_peak = mem[i, h, size : size + 1, :]
                    later_total = mem[i, h, size + 1 : size + 2, :]
                    earlier = later_total + state_peak[h, 0:1, :]
                    peak = jnp.maximum(earlier, later_peak)
                    state[h] = (
                        jnp.exp(earlier - peak) * state[h]
                        + jnp.exp(later_peak - peak) * mem[i, h, :size, :]
                    )
                    state_peak[h, 0:1, :] = peak

            return carry

        lax.fori_loop(0, n - 1, merge, 0)
        for h in range(heads):
            rest = state[h]
            for piece in range(3):
                top_part = rest.astype(jnp.bfloat16)
                state_parts[h, piece] = top_part
                rest = rest - top_part.astype(jnp.float32)

    def attend(j):
        start = pl.multiple_of(j * chunk, chunk)
        row = start + lax.broadcasted_iota(jnp.int32, (chunk, length), 0)
        causal = row >= lax.broadcasted_iota(jnp.int32, (chunk, length), 1)
        nt = (((1,), (1,)), ((), ()))
        cell_list = []
        for h in range(heads):
            cols = slice(h * size, (h + 1) * size)
            q = query_ref[pl.ds(start, chunk), cols]
            c = cum_col_ref[pl.ds(start, chunk), h : h + 1]
            within = jnp.where(causal, c - cum_ref[h : h + 1, :] + in_ref[h : h + 1, :], -jnp.inf)
            carried = c + state_peak[h, 0:1, 0:1]
            top = jnp.maximum(jnp.max(within, axis=1, keepdims=True), carried)
            raw = lax.dot_general(q, key_ref[:, cols], nt, preferred_element_type=jnp.float32)
            scores = (raw * scale * jnp.exp(within - top)).astype(jnp.bfloat16)
            cells = jnp.dot(scores, value_ref[:, cols], preferred_element_type=jnp.float32)
            held = jnp.zeros((chunk, size), jnp.float32)
            for piece in (2, 1, 0):
                held = held + lax.dot_general(
                    q, state_parts[h, piece], nt, preferred_element_type=jnp.float32
                )
            cells = cells + jnp.exp(carried - top) * held
            mean = jnp.mean(cells * cells, axis=1, keepdims=True)
            cell_list.append(
                (cells * lax.rsqrt(mean + epsilon) * gain_ref[h : h + 1, :]).astype(jnp.bfloat16)
            )
        cell_rows = jnp.concatenate(cell_list, axis=1)
        for q in range(4):
            cols = slice(q * quarter, (q + 1) * quarter)
            mpart[j, :, cols] = jnp.dot(
                cell_rows, project_ref[:, cols], preferred_element_type=jnp.float32
            ).astype(jnp.bfloat16)

    begin = n - 1

    def mixer_step(t):
        @pl.when(t == begin)
        def _():
            prefix()

        @pl.when((t >= begin) & (t < begin + 4))
        def _():
            k = t - begin
            attend(jnp.where(k == 0, pair_cross, jnp.where(k == 1, pair, jnp.where(k == 2, cross, tp))))

        @pl.when(t == begin)
        def _():
            mixed_half(1, pair_cross).start()

        @pl.when(t == begin + 1)
        def _():
            mixed_half(0, pair).start()

        @pl.when(t == begin + 3)
        def _():
            mixed_half(1, pair_cross).wait_recv()
            msum[...] = (
                mpart[cross].astype(jnp.float32) + mpin[1].astype(jnp.float32)
            ).astype(jnp.bfloat16)
            mixed_sum().start()

    lax.fori_loop(1, n, first, 0)
    lax.fori_loop(1, n, second, 0)
    own.wait()

    def source(i):
        return lax.rem(me + n - i, n)

    def step(t, carry):
        @pl.when(t < n)
        def _():
            s = source(t)

            @pl.when(t > 0)
            def _():
                scatter(t, s).wait_recv()

            across(s).start()
            beside(s, 0, tp).start()

        @pl.when((t >= 1) & (t < n + 1))
        def _():
            s = source(t - 1)
            remote(
                rows.at[s, cross], rows.at[s, cross], send_x.at[s], recv_x.at[s], (me, cross)
            ).wait_recv()
            beside(s, 1, cross).start()

        @pl.when((t >= 2) & (t < n + 2))
        def _():
            s = source(t - 2)
            beside(s, 0, pair).wait_recv()
            beside(s, 1, pair_cross).wait_recv()
            x = rows[s].reshape(cap, width)
            gate_act = jnp.dot(x, gate_ref[...], preferred_element_type=jnp.float32)
            up_act = jnp.dot(x, up_ref[...], preferred_element_type=jnp.float32)
            hidden = (gate_act * jax.nn.sigmoid(gate_act) * up_act).astype(jnp.bfloat16)
            for q in range(4):
                part[s, q] = jnp.dot(
                    hidden,
                    down_ref[:, q * quarter : (q + 1) * quarter],
                    preferred_element_type=jnp.float32,
                ).astype(jnp.bfloat16)
            halves(s, 1, pair_cross).start()
            halves(s, 0, pair).start()

        @pl.when((t >= 3) & (t < n + 3))
        def _():
            s = source(t - 3)
            halves(s, 1, pair_cross).wait_recv()
            csum[s] = (
                part[s, cross].astype(jnp.float32) + pin[s, 1].astype(jnp.float32)
            ).astype(jnp.bfloat16)
            summed(s).start()

        @pl.when(t >= 4)
        def _():
            i = t - 4
            s = source(i)
            halves(s, 0, pair).wait_recv()
            summed(s).wait_recv()
            total = (
                part[s, tp].astype(jnp.float32)
                + pin[s, 0].astype(jnp.float32)
                + xin[s].astype(jnp.float32)
            ).astype(jnp.bfloat16)

            @pl.when(i > 0)
            def _():
                fin[s] = total
                back(i).start()

            @pl.when(i == 0)
            def _():
                ret[s] = total

        mixer_step(t)
        return carry

    lax.fori_loop(0, n + 4, step, 0)

    mixed_half(0, pair).wait_recv()
    mixed_sum().wait_recv()
    mixed_ref[...] = (
        mpart[tp].astype(jnp.float32) + mpin[0].astype(jnp.float32) + mxin[...].astype(jnp.float32)
    ).astype(mixed_ref.dtype)

    def finish(i, carry):
        back(i).wait_recv()
        back(i).wait_send()
        scatter(i, me).wait_send()

        @pl.when(me + i < n)
        def _():
            memory(i).wait_send()

        return carry

    lax.fori_loop(1, n, finish, 0)
    mix = mix_ref[...]
    high = mix.astype(jnp.bfloat16)
    low = (mix - high.astype(jnp.float32)).astype(jnp.bfloat16)
    table = ret[...].reshape(n * cap, quarter)
    out_ref[...] = (
        jnp.dot(high, table, preferred_element_type=jnp.float32)
        + jnp.dot(low, table, preferred_element_type=jnp.float32)
    ).astype(out_ref.dtype)

    def drain(s, carry):
        across(s).wait_send()
        beside(s, 0, tp).wait_send()
        beside(s, 1, cross).wait_send()
        halves(s, 0, pair).wait_send()
        halves(s, 1, pair_cross).wait_send()
        summed(s).wait_send()
        return carry

    lax.fori_loop(0, n, drain, 0)
    mixed_half(0, pair).wait_send()
    mixed_half(1, pair_cross).wait_send()
    mixed_sum().wait_send()


def all_fused(own_share, gate_weight, up_weight, down_weight, mix, prepared, gain, project):
    n, share, width = own_share.shape
    cap = share * 4
    quarter = width // 4
    tokens = mix.shape[0]
    packed, queries, keys, values, cumulative, input_gate = prepared
    heads, size = packed.shape[0], packed.shape[2]
    chunk = queries.shape[0] // 4
    vmem = pl.BlockSpec(memory_space=pltpu.VMEM)
    dma = pltpu.SemaphoreType.DMA
    bf = jnp.bfloat16
    return pl.pallas_call(
        functools.partial(expert_kernel, (n, share, cap, width, quarter)),
        out_shape=(
            jax.ShapeDtypeStruct((tokens, quarter), bf),
            jax.ShapeDtypeStruct((chunk, width), bf),
        ),
        in_specs=[vmem] * 14,
        out_specs=(vmem, vmem),
        scratch_shapes=[
            pltpu.VMEM((n, 4, share, width), bf),
            pltpu.VMEM((n, 4, cap, quarter), bf),
            pltpu.VMEM((n, 2, cap, quarter), bf),
            pltpu.VMEM((n, cap, quarter), bf),
            pltpu.VMEM((n, cap, quarter), bf),
            pltpu.VMEM((n, cap, quarter), bf),
            pltpu.VMEM((n, cap, quarter), bf),
            pltpu.VMEM((n, heads, size + 8, size), jnp.float32),
            pltpu.VMEM((heads, size, size), jnp.float32),
            pltpu.VMEM((heads, 8, size), jnp.float32),
            pltpu.VMEM((heads, 3, size, size), bf),
            pltpu.VMEM((4, chunk, width), bf),
            pltpu.VMEM((2, chunk, width), bf),
            pltpu.VMEM((chunk, width), bf),
            pltpu.VMEM((chunk, width), bf),
            dma,
            dma((n,)), dma((n,)), dma((n,)), dma((n,)),
            dma((n, 2)), dma((n, 2)), dma((n, 2)), dma((n, 2)),
            dma((n,)), dma((n,)), dma((n,)), dma((n,)),
            dma((n,)), dma((n,)), dma((2,)), dma((2,)), dma, dma,
        ],
        compiler_params=pltpu.CompilerParams(collective_id=0, has_side_effects=True),
        cost_estimate=pl.CostEstimate(
            flops=60_000_000_000, bytes_accessed=8_000_000, transcendentals=0
        ),
    )(
        own_share, gate_weight, up_weight, down_weight, mix,
        packed, queries, keys, values, cumulative, cumulative.T, input_gate, gain, project,
    )


def experts_plain(own_share, gate_weight, up_weight, down_weight, mix):
    arrived = lax.all_to_all(own_share, "ep", split_axis=0, concat_axis=0, tiled=True)
    piece_rows = lax.all_gather(arrived, "tp", axis=1, tiled=True)
    gate_act = jnp.einsum(
        "scd,df->scf", piece_rows, gate_weight, preferred_element_type=jnp.float32
    )
    up_act = jnp.einsum("scd,df->scf", piece_rows, up_weight, preferred_element_type=jnp.float32)
    hidden = (jax.nn.silu(gate_act) * up_act).astype(jnp.bfloat16)
    partial_rows = jnp.einsum(
        "scf,fo->sco", hidden, down_weight, preferred_element_type=jnp.float32
    )
    summed = lax.psum_scatter(
        partial_rows.astype(jnp.bfloat16), "tp", scatter_dimension=2, tiled=True
    )
    returned = lax.all_to_all(summed, "ep", split_axis=0, concat_axis=0, tiled=True)
    return jnp.dot(
        mix, returned.reshape(-1, returned.shape[2]).astype(jnp.float32), precision=highest
    ).astype(jnp.bfloat16)


def mixer_prepare(normed_a, query_weight, key_weight, value_weight, input_gate, forget_gate):
    def project(weight):
        return jnp.dot(normed_a, weight, preferred_element_type=jnp.float32).astype(jnp.bfloat16)

    rows = normed_a.shape[0]
    heads = input_gate.shape[0]
    width_local = query_weight.shape[1]
    head_size = width_local // heads
    scale = head_size ** (-0.5)
    causal = jnp.tril(jnp.ones((rows, rows), dtype=bool))
    log_forget = jax.nn.log_sigmoid(forget_gate)
    cumulative = jnp.einsum(
        "hs,ts->ht", log_forget, causal.astype(jnp.float32), precision=highest
    )
    total = cumulative[:, -1]
    log_weight = total[:, None] - cumulative + input_gate
    peak = jnp.max(log_weight, axis=-1)
    weights = jnp.exp(log_weight - peak[:, None])
    keys = project(key_weight)
    values = project(value_weight)

    def by_head(matrix):
        return [matrix[:, h * head_size : (h + 1) * head_size] for h in range(heads)]

    key_heads, value_heads = by_head(keys), by_head(values)
    memory = jnp.stack(
        [
            lax.dot_general(
                value_heads[h].astype(jnp.float32) * weights[h][:, None],
                key_heads[h].astype(jnp.float32) * scale,
                (((0,), (0,)), ((), ())),
                precision=highest,
            )
            for h in range(heads)
        ]
    )
    stats = jnp.stack([peak, total], axis=1)
    stats = jnp.concatenate([stats, jnp.zeros((heads, 6), jnp.float32)], axis=1)
    packed = jnp.concatenate(
        [memory, jnp.broadcast_to(stats[:, :, None], (heads, 8, head_size))], axis=1
    )
    return (packed, project(query_weight), keys, values, cumulative, input_gate)


def mixer_partial(prepared, gain_local, mixer_out_weight):
    packed, queries, keys, values, cumulative, input_gate = prepared
    rows = queries.shape[0]
    heads, head_size = gain_local.shape
    scale = head_size ** (-0.5)
    causal = jnp.tril(jnp.ones((rows, rows), dtype=bool))

    def by_head(matrix):
        return [matrix[:, h * head_size : (h + 1) * head_size] for h in range(heads)]

    query_heads, key_heads, value_heads = by_head(queries), by_head(keys), by_head(values)
    everything = lax.all_gather(packed, "ep")
    n, place = lax.axis_size("ep"), lax.axis_index("ep")
    peaks = everything[:, :, head_size, 0]
    totals = everything[:, :, head_size + 1, 0]
    order = jnp.arange(n)
    later = (order[None, :] > order[:, None]) & (order[None, :] < place)
    suffix = jnp.sum(jnp.where(later[:, :, None], totals[None], 0.0), axis=1)
    before = (order < place)[:, None]
    candidate = jnp.where(before, peaks + suffix, floor_log)
    state_peak = jnp.max(candidate, axis=0)
    fade = jnp.where(before, jnp.exp(candidate - state_peak[None]), 0.0)
    state = jnp.sum(everything[:, :, :head_size] * fade[:, :, None, None], axis=0)
    cell_list = []
    for h in range(heads):
        c, gate = cumulative[h], input_gate[h]
        within = jnp.where(causal, c[:, None] - c[None, :] + gate[None, :], -jnp.inf)
        carried = c + state_peak[h]
        top = jnp.maximum(jnp.max(within, axis=-1), carried)
        raw = lax.dot_general(
            query_heads[h], key_heads[h], (((1,), (1,)), ((), ())), preferred_element_type=jnp.float32
        )
        scores = raw * scale * jnp.exp(within - top[:, None])
        cells = jnp.dot(
            scores.astype(jnp.bfloat16), value_heads[h], preferred_element_type=jnp.float32
        )
        carried_cells = lax.dot_general(
            query_heads[h].astype(jnp.float32),
            state[h],
            (((1,), (1,)), ((), ())),
            precision=highest,
        )
        cells = cells + jnp.exp(carried - top)[:, None] * carried_cells
        cell_list.append(rms_rows(cells, gain_local[h]).astype(jnp.bfloat16))
    cell_rows = jnp.concatenate(cell_list, axis=1)
    return jnp.dot(cell_rows, mixer_out_weight, preferred_element_type=jnp.float32).astype(
        jnp.bfloat16
    )


def shards(
    mixer_in,
    mixer_gain,
    query_weight,
    key_weight,
    value_weight,
    input_gate,
    forget_gate,
    head_gain,
    mixer_out_weight,
    expert_in,
    expert_gain,
    group_router,
    expert_router,
    routes,
    gate_experts,
    up_experts,
    down_experts,
):
    normed_b = rms_rows(expert_in, expert_gain).astype(jnp.bfloat16)
    tokens = normed_b.shape[0]
    expert_total = expert_router.shape[1]
    members = expert_total // group_router.shape[1]
    capacity = 4 * tokens // expert_total
    share = capacity // lax.axis_size("tp")
    group_logits = jnp.dot(normed_b, group_router, preferred_element_type=jnp.float32)
    expert_logits = jnp.dot(normed_b, expert_router, preferred_element_type=jnp.float32)
    expert_ids = jnp.arange(expert_total, dtype=jnp.int32)
    group_ids = jnp.arange(group_router.shape[1], dtype=jnp.int32)
    named = [routes[:, k : k + 1] == expert_ids[None, :] for k in range(2)]
    chosen = [jnp.sum(jnp.where(m, expert_logits, 0.0), axis=1, keepdims=True) for m in named]
    combine = jnp.zeros((tokens, expert_total), jnp.float32)
    for k in range(2):
        in_group = routes[:, k : k + 1] // members == group_ids[None, :]
        group_pick = jnp.sum(jnp.where(in_group, group_logits, 0.0), axis=1, keepdims=True)
        weight = jax.nn.sigmoid(group_pick) * jax.nn.sigmoid(chosen[k] - chosen[1 - k])
        combine = combine + jnp.where(named[k], weight, 0.0)
    matches = named[0] | named[1]
    earlier = jnp.tril(jnp.ones((tokens, tokens), jnp.bfloat16), -1)
    rank = jnp.dot(
        earlier, matches.astype(jnp.bfloat16), preferred_element_type=jnp.float32
    ).astype(jnp.int32)
    rank = jnp.where(matches, rank, -1)
    slots = jnp.arange(capacity, dtype=jnp.int32)
    mix = jnp.where(
        rank[:, :, None] == slots[None, None, :], combine[:, :, None], 0.0
    ).reshape(tokens, expert_total * capacity)
    own_slots = lax.axis_index("tp") * share + jnp.arange(share, dtype=jnp.int32)
    select = (rank.T[:, None, :] == own_slots[None, :, None]).astype(jnp.bfloat16)
    own_share = (
        jnp.dot(
            select.reshape(expert_total * share, tokens),
            normed_b,
            preferred_element_type=jnp.float32,
        )
        .astype(jnp.bfloat16)
        .reshape(expert_total, share, normed_b.shape[1])
    )
    normed_a = rms_rows(mixer_in, mixer_gain).astype(jnp.bfloat16)
    prepared = mixer_prepare(
        normed_a, query_weight, key_weight, value_weight, input_gate, forget_gate
    )
    width_local = query_weight.shape[1]
    gain_local = lax.dynamic_slice_in_dim(
        head_gain, lax.axis_index("tp") * width_local, width_local
    ).reshape(input_gate.shape[0], -1)
    experts = (own_share, gate_experts[0], up_experts[0], down_experts[0], mix)
    fused = lax.axis_size("tp") == 4 and share % 16 == 0 and lax.axis_size("ep") > 1
    if fused and mixer_in.shape[0] % 512 == 0:
        expert_out, mixer_out = all_fused(*experts, prepared, gain_local, mixer_out_weight)
    else:
        partial = mixer_partial(prepared, gain_local, mixer_out_weight)
        mixer_out = lax.psum_scatter(partial, "tp", scatter_dimension=0, tiled=True)
        expert_out = experts_plain(*experts)
    return (mixer_out, expert_out)


def solution(mesh):
    in_specs = (
        P("ep", None),
        P(),
        P(None, "tp"),
        P(None, "tp"),
        P(None, "tp"),
        P("tp", "ep"),
        P("tp", "ep"),
        P(),
        P("tp", None),
        P("ep", None),
        P(),
        P(),
        P(),
        P("ep", None),
        P("ep", None, "tp"),
        P("ep", None, "tp"),
        P("ep", "tp", None),
    )
    out_specs = (P(("ep", "tp"), None), P("ep", "tp"))
    return jax.shard_map(shards, mesh=mesh, in_specs=in_specs, out_specs=out_specs, check_vma=False)
```

profile of v0, /device:TPU:0, one launch (start us, length us, event | category | flops | bytes accessed | tf_op | source)
XLA Modules:
  0.0 116.3 jit_solution(12332587474756145078)
XLA Ops:
  0.6 0.0 copy-start
  0.6 0.0 copy-start.3
  0.7 0.0 copy-start.8
  0.7 0.0 copy-start.7
  0.7 0.9 and_select_fusion
  1.5 1.5 %fusion.3 = f32[256]{0:T(256)S(1)} fusion(bf16[256,2048]{1,0:T(8,128)(2,1)} %param.26), kind=kLoop, calls=%fused_computation.8 | loop fusion | flops 1572608 | bytes 1049600 | tf_op jit(solution)/shard_map/reduce_sum | solution.py:20
  3.1 1.7 %select_reduce_fusion.1 = (f32[256]{0:T(256)S(1)}, f32[256]{0:T(256)S(1)}) fusion(s32[256]{0:T(256)S(1)} %bitcast.45, s32[256]{0:T(256)S(1)} %bitcast.41, bf16[2048,8]{0,1:T(8,128)(2,1)} %param.29, bf16[256,2048]{1,0:T(8,128)(2,1)} %param.26, f32[2048]{0:T(1024)} %param.27, f32[256]{0:T(256)S(1)} %add_rsqrt_fusion.1), kind=kOutput, calls=%fused_computation.48 | convolution fusion | flops 10497536 | bytes 1094656 | tf_op jit(solution)/shard_map/dot_general | solution.py:511
  4.8 0.0 copy-done.3
  4.8 0.0 copy-done.8
  4.8 0.5 fusion.43
  5.3 0.1 copy.24
  5.4 0.3 broadcast_in_dim.90
  5.8 0.2 bitcast_select_fusion.1
  6.1 0.1 copy.23
  6.2 0.0 copy-start.10
  6.2 0.0 copy-start.5
  6.2 0.0 copy-start.1
  6.2 0.3 eq.142
  6.6 0.0 copy-start.9
  6.6 1.5 %bitcast_select_fusion.mix_ref = f32[256,1024]{1,0:T(8,128)} fusion(f32[32,8,8,128]{3,2,1,0:T(8,128)S(1)} %bitcast.38, s32[32,8,8,128]{3,2,1,0:T(8,128)S(1)} %bitcast.39, s32[1024]{0:T(1024)S(1)} %iota_bitcast_fusion), kind=kLoop, calls=%fused_computation.17 | loop fusion | flops 524288 | bytes 3149824 | tf_op jit(solution)/shard_map/jit(_where)/select_n | solution.py:529
  8.1 0.4 fusion.6.cum_ref
  8.5 0.2 slice_reduce_fusion
  8.8 0.0 copy-done.5
  8.8 0.2 fusion.59
  9.0 0.1 subtract_exponential_fusion
  9.1 0.5 fusion
  9.6 0.0 copy-start.6
  9.6 0.8 convolution_convert_fusion.2.key_ref
  10.4 0.4 copy-done.6
  10.8 0.8 convolution_convert_fusion.3.value_ref
  11.6 0.0 copy-start.2
  11.6 0.7 convolution_bitcast_fusion
  12.3 0.0 copy-done.11
  12.3 0.7 convolution_bitcast_fusion.1
  13.0 0.1 copy.25
  13.1 0.1 pad.5.clone
  13.2 0.1 maximum_maximum_fusion
  13.3 0.1 broadcast_in_dim.94
  13.3 0.7 pad_maximum_fusion.packed_ref
  14.0 0.1 eq.139
  14.1 0.1 bitcast_compare_fusion.1
  14.2 2.8 %convolution_convert_fusion = bf16[256,2048]{1,0:T(8,128)(2,1)} fusion(pred[256,256]{1,0:T(32,128)(4,1)S(1)} %bitcast_compare_fusion.1, bf16[256,2048]{1,0:T(8,128)(2,1)} %param.26, f32[2048]{0:T(1024)S(1)} %copy-done.8, f32[256]{0:T(256)S(1)} %add_rsqrt_fusion.1), kind=kOutput, calls=%fused_computation.7 | convolution fusion | flops 271056896 | bytes 2171904 | tf_op jit(solution)/shard_map/dot_general | solution.py:535
  17.0 1.3 %dynamic-slice_bitcast_fusion.gain_ref = f32[2,128]{1,0:T(2,128)} fusion(f32[1024]{0:T(1024)} %param.24, s32[]{:T(128)S(6)} %select_n.76), kind=kLoop, calls=%fused_computation.86 | loop fusion | bytes 2052 | tf_op jit(solution)/shard_map/reshape | solution.py:550
  18.3 0.9 copy.26
  19.2 2.7 %convolution_convert_fusion.1.query_ref = bf16[512,256]{1,0:T(8,128)(2,1)} fusion(bf16[2048,256]{1,0:T(8,128)(2,1)} %param.19, bf16[512,2048]{1,0:T(8,128)(2,1)S(1)} %copy-done.2, f32[2048]{0:T(1024)S(1)} %copy-done.9, f32[512]{0:T(512)S(1)} %add_rsqrt_fusion), kind=kOutput, calls=%fused_computation.11 | convolution fusion | flops 541196288 | bytes 3418112 | tf_op jit(solution)/shard_map/dot_general | solution.py:393
  21.9 90.9 %shard_map.176 = (bf16[256,512]{1,0:T(8,128)(2,1)}, bf16[128,2048]{1,0:T(8,128)(2,1)}) custom-call(bf16[8,32,2048]{2,1,0:T(8,128)(2,1)} %bitcast.57, bf16[2048,256]{1,0:T(8,128)(2,1)} %bitcast.54, bf16[2048,256]{1,0:T(8,128)(2,1)} %bitcast.55, bf16[256,2048]{1,0:T(8,128)(2,1)} %bitcast.56, f32[256,1024]{1,0:T(8,128)} %bitcast_select_fusion.mix_ref, ...), custom_call_target="tpu_custom_call" | custom-call | flops 60000002048 | bytes 8000000 | tf_op jit(solution)/shard_map/pallas_call | solution.py:331
  112.7 1.9 %copy.37 = bf16[128,2048]{1,0:T(8,128)(2,1)} copy(bf16[128,2048]{1,0:T(8,128)(2,1)} %get-tuple-element.26) | data formatting | bytes 1048576
  114.6 1.7 %copy.38 = bf16[256,512]{1,0:T(8,128)(2,1)} copy(bf16[256,512]{1,0:T(8,128)(2,1)} %get-tuple-element.27) | data formatting | bytes 524288
  (22 shorter events, 0.1 us)
Async XLA Ops:
  0.6 8.9 %copy-start = (bf16[2048,256]{1,0:T(8,128)(2,1)S(1)}, bf16[2048,256]{1,0:T(8,128)(2,1)}, u32[]{:S(2)}) copy-start(bf16[2048,256]{1,0:T(8,128)(2,1)} %param.20) | copy-start | bytes 3145732
  0.6 4.1 %copy-start.3 = (bf16[256,2048]{1,0:T(8,128)(2,1)S(1)}, bf16[256,2048]{1,0:T(8,128)(2,1)}, u32[]{:S(2)}) copy-start(bf16[256,2048]{1,0:T(8,128)(2,1)} %param.26) | copy-start | bytes 3145732
  0.7 4.1 %copy-start.8 = (f32[2048]{0:T(1024)S(1)}, f32[2048]{0:T(1024)}, u32[]{:S(2)}) copy-start(f32[2048]{0:T(1024)} %param.27) | copy-start | bytes 24580
  0.7 4.1 %copy-start.7 = (bf16[2048,2]{0,1:T(2,128)(2,1)S(1)}, bf16[2048,2]{0,1:T(2,128)(2,1)}, u32[]{:S(2)}) copy-start(bf16[2048,2]{0,1:T(2,128)(2,1)} %param.28) | copy-start | bytes 24580
  6.2 1.9 %copy-start.10 = (f32[2,512]{1,0:T(2,128)S(1)}, f32[2,512]{1,0:T(2,128)}, u32[]{:S(2)}) copy-start(f32[2,512]{1,0:T(2,128)} %param.23) | copy-start | bytes 12292
  6.2 2.6 %copy-start.5 = (f32[2,512]{1,0:T(2,128)S(1)}, f32[2,512]{1,0:T(2,128)}, u32[]{:S(2)}) copy-start(f32[2,512]{1,0:T(2,128)} %in_ref.1) | copy-start | bytes 12292
  6.2 2.8 %copy-start.1 = (bf16[512,2048]{1,0:T(8,128)(2,1)S(1)}, bf16[512,2048]{1,0:T(8,128)(2,1)}, u32[]{:S(2)}) copy-start(bf16[512,2048]{1,0:T(8,128)(2,1)} %param.17) | copy-start | bytes 6291460
  6.6 3.0 %copy-start.9 = (f32[2048]{0:T(1024)S(1)}, f32[2048]{0:T(1024)}, u32[]{:S(2)}) copy-start(f32[2048]{0:T(1024)} %param.18) | copy-start | bytes 24580
  8.5 9.8 %copy-start.4 = (f32[2,512]{1,0:T(2,128)}, f32[2,512]{1,0:T(2,128)S(1)}, u32[]{:S(2)}) copy-start(f32[2,512]{1,0:T(2,128)S(1)} %fusion.6.cum_ref) | copy-start | bytes 12292
  9.6 1.2 %copy-start.6 = (bf16[2048,256]{1,0:T(8,128)(2,1)S(1)}, bf16[2048,256]{1,0:T(8,128)(2,1)}, u32[]{:S(2)}) copy-start(bf16[2048,256]{1,0:T(8,128)(2,1)} %param.21) | copy-start | bytes 3145732
  10.8 1.5 %copy-start.11 = (bf16[512,256]{1,0:T(8,128)(2,1)}, bf16[512,256]{1,0:T(8,128)(2,1)S(1)}, u32[]{:S(2)}) copy-start(bf16[512,256]{1,0:T(8,128)(2,1)S(1)} %convolution_convert_fusion.2.key_ref) | copy-start | bytes 786436
  11.6 1.4 %copy-start.12 = (bf16[512,256]{1,0:T(8,128)(2,1)}, bf16[512,256]{1,0:T(8,128)(2,1)S(1)}, u32[]{:S(2)}) copy-start(bf16[512,256]{1,0:T(8,128)(2,1)S(1)} %convolution_convert_fusion.3.value_ref) | copy-start | bytes 786436
  11.6 7.6 %copy-start.2 = (bf16[512,2048]{1,0:T(8,128)(2,1)S(1)}, bf16[512,2048]{1,0:T(8,128)(2,1)}, u32[]{:S(2)}) copy-start(bf16[512,2048]{1,0:T(8,128)(2,1)} %param.17) | copy-start | bytes 6291460
where the time goes:
time: 119 us; the launch traced here: 116 us
  Pallas kernels  90.9 us (76%)
  matrix products  11.2 us (9%)
  local copies, waits for them, and re-layouts  7.7 us (6%)
  other arithmetic  5.59 us (5%)
    pallas_call x1, Pallas kernels, all_fused(): pl.pallas_call(functools.partial(expert_kernel, (n, share, cap, width, qu...  90.9 us
    dot_general x3, matrix products, project(): jnp.dot(normed_a, weight, preferred_element_type=jnp.float32)  4.24 us
    unnamed x28, local copies, waits for them, and re-layouts  4.04 us
    dot_general x1, matrix products, shards(): jnp.dot(select.reshape(expert_total * share, tokens), normed_b, preferred...  2.78 us

commit v1 on v0

--- a/solution.py
+++ b/solution.py
@@ -15,10 +15,20 @@
 floor_log = -1e30
 
 
+def is_power(count):
+    return count & (count - 1) == 0
+
+
 def rms_rows(matrix, gain):
     widened = matrix.astype(jnp.float32)
     scaled = widened * lax.rsqrt(jnp.mean(widened * widened, axis=-1, keepdims=True) + epsilon)
     return scaled * gain
+
+
+def merged(earlier_memory, earlier_peak, later_memory, later_peak, later_total):
+    moved = later_total + earlier_peak
+    peak = jnp.maximum(moved, later_peak)
+    return jnp.exp(moved - peak) * earlier_memory + jnp.exp(later_peak - peak) * later_memory, peak
 
 
 def expert_kernel(
@@ -26,16 +36,36 @@
     packed_ref, query_ref, key_ref, value_ref, cum_ref, cum_col_ref, in_ref, gain_ref, project_ref,
     out_ref, mixed_ref,
     rows, part, pin, csum, xin, fin, ret,
-    mem, state, state_peak, state_parts, mpart, mpin, msum, mxin,
+    peer, plane, mem, pre, pre_in, state, state_peak, state_parts, mpart, mpin, msum, mxin,
     own_sem, send_a, recv_a, send_x, recv_x, send_p, recv_p,
     send_q, recv_q, send_c, recv_c, send_r, recv_r,
-    send_m, recv_m, send_h, recv_h, send_y, recv_y,
+    send_m, recv_m, send_k, recv_k, send_h, recv_h, send_y, recv_y,
 ):
     n, share, cap, width, quarter = sizes
+    near = n // 2
+    planes = n // 2
     me, tp = lax.axis_index("ep"), lax.axis_index("tp")
-    pair = tp + 1 - 2 * lax.rem(tp, 2)
+    core, column = lax.rem(tp, 2), lax.div(tp, 2)
+    pair = tp + 1 - 2 * core
     cross = lax.rem(tp + 2, 4)
     pair_cross = lax.rem(pair + 2, 4)
+    side, level = lax.rem(me, 2), lax.div(me, 2)
+    mate = me + 1 - 2 * side
+
+    def other(i):
+        total, bit = 0, 1
+        while bit < n:
+            total = total + bit * lax.rem(lax.div(me, bit) + lax.div(i, bit), 2)
+            bit *= 2
+        return total
+
+    high = lax.rem(lax.div(me, near), 2)
+    inner = lax.rem(high + lax.div(lax.rem(me, near), near // 2), 2)
+
+    def turn(t):
+        half = near // 2
+        swapped = near + lax.rem(t - near + inner * half, near)
+        return jnp.where(t < near, t, swapped)
 
     def remote(src, dst, send, recv, to):
         return pltpu.make_async_remote_copy(
@@ -49,20 +79,30 @@
         )
     pl.semaphore_signal(barrier, inc=1, device_id=(me, pair), device_id_type=MESH)
     pl.semaphore_signal(barrier, inc=1, device_id=(me, cross), device_id_type=MESH)
-    own = pltpu.make_async_copy(own_ref.at[me], rows.at[me, tp], own_sem)
+    own = pltpu.make_async_copy(own_ref.at[me], rows.at[me, core], own_sem)
     own.start()
     pl.semaphore_wait(barrier, n + 1)
 
-    def scatter(i, place):
-        to = lax.rem(me + i, n)
-        return remote(own_ref.at[to], rows.at[place, tp], send_a.at[i], recv_a.at[i], (to, tp))
-
-    def across(s):
-        return remote(rows.at[s, tp], rows.at[s, tp], send_x.at[s], recv_x.at[s], (me, cross))
-
-    def beside(s, k, who):
+    def scatter_near(i, place):
+        to = other(i)
+        return remote(own_ref.at[to], rows.at[place, core], send_a.at[i], recv_a.at[i], (to, tp))
+
+    def scatter_far(i, place):
+        to = other(i)
+        mine = pl.ds(pl.multiple_of(column * share, share), share)
         return remote(
-            rows.at[s, who], rows.at[s, who], send_p.at[s, k], recv_p.at[s, k], (me, pair)
+            own_ref.at[to, mine], rows.at[place, core, mine], send_a.at[i], recv_a.at[i], (to, tp)
+        )
+
+    def across(s, which):
+        mine = pl.ds(pl.multiple_of(which * share, share), share)
+        return remote(
+            rows.at[s, core, mine], rows.at[s, core, mine], send_x.at[s], recv_x.at[s], (me, cross)
+        )
+
+    def beside(s, which):
+        return remote(
+            rows.at[s, which], rows.at[s, which], send_p.at[s], recv_p.at[s], (me, pair)
         )
 
     def halves(s, k, who):
@@ -72,61 +112,99 @@
         return remote(csum.at[s], xin.at[s], send_c.at[s], recv_c.at[s], (me, cross))
 
     def back(i):
-        to = lax.rem(me + n - i, n)
+        to = other(i)
         return remote(fin.at[to], ret.at[me], send_r.at[i], recv_r.at[i], (to, tp))
 
-    def memory(i):
+    def to_mate():
+        return remote(packed_ref, peer, send_k.at[0], recv_k.at[0], (mate, tp))
+
+    def to_level(d):
         return remote(
-            packed_ref, mem.at[i], send_m.at[i], recv_m.at[i], (lax.rem(me + i, n), tp)
-        )
+            plane, mem.at[level], send_m.at[d], recv_m.at[d], (lax.rem(me + 2 * d, n), tp)
+        )
+
+    def from_level(d):
+        return remote(
+            plane, mem.at[level - d], send_m.at[d], recv_m.at[d], (lax.rem(me + 2 * d, n), tp)
+        )
+
+    def prefix_mate():
+        return remote(pre, pre_in, send_k.at[1], recv_k.at[1], (mate, tp))
 
     def mixed_half(k, who):
         return remote(mpart.at[who], mpin.at[k], send_h.at[k], recv_h.at[k], (me, pair))
 
     def mixed_sum():
         return remote(msum, mxin, send_y, recv_y, (me, cross))
-
-    def first(i, carry):
-        scatter(i, me).start()
-        return carry
-
-    def second(i, carry):
-        @pl.when(me + i < n)
-        def _():
-            memory(i).start()
-
-        return carry
 
     heads = packed_ref.shape[0]
     size = packed_ref.shape[2]
     length = query_ref.shape[0]
     chunk = length // 4
     scale = size ** (-0.5)
-
-    def prefix():
-        state[...] = jnp.zeros_like(state)
-        state_peak[...] = jnp.full_like(state_peak, floor_log)
-
-        def merge(k, carry):
-            i = n - 1 - k
-
-            @pl.when(i <= me)
+    body, top_row, sum_row = slice(0, size), slice(size, size + 1), slice(size + 1, size + 2)
+
+    def combine_plane():
+        to_mate().wait_recv()
+
+        def joined(first, second):
+            memory, peak = merged(
+                first[side, body], first[side, top_row],
+                second[side, body], second[side, top_row], second[side, sum_row],
+            )
+            plane[size : size + 8] = jnp.zeros((8, size), jnp.float32)
+            plane[body] = memory
+            plane[top_row] = peak
+            plane[sum_row] = first[side, sum_row] + second[side, sum_row]
+
+        @pl.when(side == 0)
+        def _():
+            joined(packed_ref, peer)
+
+        @pl.when(side == 1)
+        def _():
+            joined(peer, packed_ref)
+
+        for d in range(1, planes):
+            @pl.when(level + d < planes)
             def _():
-                memory(i).wait_recv()
-                for h in range(heads):
-                    later_peak = mem[i, h, size : size + 1, :]
-                    later_total = mem[i, h, size + 1 : size + 2, :]
-                    earlier = later_total + state_peak[h, 0:1, :]
-                    peak = jnp.maximum(earlier, later_peak)
-                    state[h] = (
-                        jnp.exp(earlier - peak) * state[h]
-                        + jnp.exp(later_peak - peak) * mem[i, h, :size, :]
-                    )
-                    state_peak[h, 0:1, :] = peak
-
-            return carry
-
-        lax.fori_loop(0, n - 1, merge, 0)
+                to_level(d).start()
+
+    def combine_levels():
+        pre[...] = jnp.zeros_like(pre)
+        pre[top_row] = jnp.full((1, size), floor_log, jnp.float32)
+        for k in range(planes - 1):
+            d = planes - 1 - k
+
+            @pl.when(d <= level)
+            def _():
+                from_level(d).wait_recv()
+                z = level - d
+                memory, peak = merged(
+                    pre[body], pre[top_row], mem[z, body], mem[z, top_row], mem[z, sum_row]
+                )
+                pre[body] = memory
+                pre[top_row] = peak
+
+        prefix_mate().start()
+
+    def combine_last():
+        prefix_mate().wait_recv()
+        state[side] = pre[body]
+        state_peak[side, 0:1, :] = pre[top_row]
+        state[1 - side] = pre_in[body]
+        state_peak[1 - side, 0:1, :] = pre_in[top_row]
+
+        @pl.when(side == 1)
+        def _():
+            for h in range(heads):
+                memory, peak = merged(
+                    state[h], state_peak[h, 0:1, :],
+                    peer[h, body], peer[h, top_row], peer[h, sum_row],
+                )
+                state[h] = memory
+                state_peak[h, 0:1, :] = peak
+
         for h in range(heads):
             rest = state[h]
             for piece in range(3):
@@ -167,12 +245,16 @@
                 cell_rows, project_ref[:, cols], preferred_element_type=jnp.float32
             ).astype(jnp.bfloat16)
 
-    begin = n - 1
+    begin = 4
 
     def mixer_step(t):
+        @pl.when(t == 2)
+        def _():
+            combine_levels()
+
         @pl.when(t == begin)
         def _():
-            prefix()
+            combine_last()
 
         @pl.when((t >= begin) & (t < begin + 4))
         def _():
@@ -187,7 +269,7 @@
         def _():
             mixed_half(0, pair).start()
 
-        @pl.when(t == begin + 3)
+        @pl.when(t == begin + 2)
         def _():
             mixed_half(1, pair_cross).wait_recv()
             msum[...] = (
@@ -195,38 +277,76 @@
             ).astype(jnp.bfloat16)
             mixed_sum().start()
 
-    lax.fori_loop(1, n, first, 0)
-    lax.fori_loop(1, n, second, 0)
+    def first_near(i, carry):
+        scatter_near(i, me).start()
+        return carry
+
+    def first_far(t, carry):
+        scatter_far(turn(t), me).start()
+        return carry
+
+    to_mate().start()
+    lax.fori_loop(1, near - 1, first_near, 0)
     own.wait()
-
-    def source(i):
-        return lax.rem(me + n - i, n)
+    beside(me, core).start()
+    combine_plane()
+    lax.fori_loop(near - 1, near, first_near, 0)
+    lax.fori_loop(near, n, first_far, 0)
 
     def step(t, carry):
-        @pl.when(t < n)
-        def _():
-            s = source(t)
-
-            @pl.when(t > 0)
+        @pl.when(t >= 4)
+        def _():
+            i = turn(t - 4)
+            s = other(i)
+            halves(s, 0, pair).wait_recv()
+            summed(s).wait_recv()
+            total = (
+                part[s, tp].astype(jnp.float32)
+                + pin[s, 0].astype(jnp.float32)
+                + xin[s].astype(jnp.float32)
+            ).astype(jnp.bfloat16)
+
+            @pl.when(i > 0)
             def _():
-                scatter(t, s).wait_recv()
-
-            across(s).start()
-            beside(s, 0, tp).start()
-
-        @pl.when((t >= 1) & (t < n + 1))
-        def _():
-            s = source(t - 1)
-            remote(
-                rows.at[s, cross], rows.at[s, cross], send_x.at[s], recv_x.at[s], (me, cross)
-            ).wait_recv()
-            beside(s, 1, cross).start()
+                fin[s] = total
+                back(i).start()
+
+            @pl.when(i == 0)
+            def _():
+                ret[s] = total
+
+        @pl.when((t >= 3) & (t < n + 3))
+        def _():
+            s = other(turn(t - 3))
+            halves(s, 1, pair_cross).wait_recv()
+            csum[s] = (
+                part[s, cross].astype(jnp.float32) + pin[s, 1].astype(jnp.float32)
+            ).astype(jnp.bfloat16)
+            summed(s).start()
+
+        @pl.when((t >= 1) & (t < near))
+        def _():
+            s = other(t)
+            scatter_near(t, s).wait_recv()
+            beside(s, core).start()
+
+        @pl.when((t >= near) & (t < n))
+        def _():
+            i = turn(t)
+            s = other(i)
+            scatter_far(i, s).wait_recv()
+            across(s, column).start()
+
+        @pl.when((t >= near + 1) & (t < n + 1))
+        def _():
+            s = other(turn(t - 1))
+            across(s, 1 - column).wait_recv()
+            beside(s, core).start()
 
         @pl.when((t >= 2) & (t < n + 2))
         def _():
-            s = source(t - 2)
-            beside(s, 0, pair).wait_recv()
-            beside(s, 1, pair_cross).wait_recv()
+            s = other(turn(t - 2))
+            beside(s, 1 - core).wait_recv()
             x = rows[s].reshape(cap, width)
             gate_act = jnp.dot(x, gate_ref[...], preferred_element_type=jnp.float32)
             up_act = jnp.dot(x, up_ref[...], preferred_element_type=jnp.float32)
@@ -240,36 +360,6 @@
             halves(s, 1, pair_cross).start()
             halves(s, 0, pair).start()
 
-        @pl.when((t >= 3) & (t < n + 3))
-        def _():
-            s = source(t - 3)
-            halves(s, 1, pair_cross).wait_recv()
-            csum[s] = (
-                part[s, cross].astype(jnp.float32) + pin[s, 1].astype(jnp.float32)
-            ).astype(jnp.bfloat16)
-            summed(s).start()
-
-        @pl.when(t >= 4)
-        def _():
-            i = t - 4
-            s = source(i)
-            halves(s, 0, pair).wait_recv()
-            summed(s).wait_recv()
-            total = (
-                part[s, tp].astype(jnp.float32)
-                + pin[s, 0].astype(jnp.float32)
-                + xin[s].astype(jnp.float32)
-            ).astype(jnp.bfloat16)
-
-            @pl.when(i > 0)
-            def _():
-                fin[s] = total
-                back(i).start()
-
-            @pl.when(i == 0)
-            def _():
-                ret[s] = total
-
         mixer_step(t)
         return carry
 
@@ -283,42 +373,55 @@
 
     def finish(i, carry):
         back(i).wait_recv()
-        back(i).wait_send()
-        scatter(i, me).wait_send()
-
-        @pl.when(me + i < n)
-        def _():
-            memory(i).wait_send()
-
         return carry
 
     lax.fori_loop(1, n, finish, 0)
     mix = mix_ref[...]
-    high = mix.astype(jnp.bfloat16)
-    low = (mix - high.astype(jnp.float32)).astype(jnp.bfloat16)
+    high_mix = mix.astype(jnp.bfloat16)
+    low_mix = (mix - high_mix.astype(jnp.float32)).astype(jnp.bfloat16)
     table = ret[...].reshape(n * cap, quarter)
     out_ref[...] = (
-        jnp.dot(high, table, preferred_element_type=jnp.float32)
-        + jnp.dot(low, table, preferred_element_type=jnp.float32)
+        jnp.dot(high_mix, table, preferred_element_type=jnp.float32)
+        + jnp.dot(low_mix, table, preferred_element_type=jnp.float32)
     ).astype(out_ref.dtype)
 
-    def drain(s, carry):
-        across(s).wait_send()
-        beside(s, 0, tp).wait_send()
-        beside(s, 1, cross).wait_send()
+    def drain(i, carry):
+        s = other(i)
+        beside(s, core).wait_send()
         halves(s, 0, pair).wait_send()
         halves(s, 1, pair_cross).wait_send()
         summed(s).wait_send()
+
+        @pl.when(i > 0)
+        def _():
+            back(i).wait_send()
+
+        @pl.when((i > 0) & (i < near))
+        def _():
+            scatter_near(i, me).wait_send()
+
+        @pl.when(i >= near)
+        def _():
+            scatter_far(i, me).wait_send()
+            across(s, column).wait_send()
+
         return carry
 
     lax.fori_loop(0, n, drain, 0)
+    to_mate().wait_send()
+    prefix_mate().wait_send()
+    for d in range(1, planes):
+        @pl.when(level + d < planes)
+        def _():
+            to_level(d).wait_send()
     mixed_half(0, pair).wait_send()
     mixed_half(1, pair_cross).wait_send()
     mixed_sum().wait_send()
 
 
 def all_fused(own_share, gate_weight, up_weight, down_weight, mix, prepared, gain, project):
-    n, share, width = own_share.shape
+    n, pieces, width = own_share.shape
+    share = pieces // 2
     cap = share * 4
     quarter = width // 4
     tokens = mix.shape[0]
@@ -328,6 +431,7 @@
     vmem = pl.BlockSpec(memory_space=pltpu.VMEM)
     dma = pltpu.SemaphoreType.DMA
     bf = jnp.bfloat16
+    f32 = jnp.float32
     return pl.pallas_call(
         functools.partial(expert_kernel, (n, share, cap, width, quarter)),
         out_shape=(
@@ -337,26 +441,29 @@
         in_specs=[vmem] * 14,
         out_specs=(vmem, vmem),
         scratch_shapes=[
-            pltpu.VMEM((n, 4, share, width), bf),
+            pltpu.VMEM((n, 2, 2 * share, width), bf),
             pltpu.VMEM((n, 4, cap, quarter), bf),
             pltpu.VMEM((n, 2, cap, quarter), bf),
             pltpu.VMEM((n, cap, quarter), bf),
             pltpu.VMEM((n, cap, quarter), bf),
             pltpu.VMEM((n, cap, quarter), bf),
             pltpu.VMEM((n, cap, quarter), bf),
-            pltpu.VMEM((n, heads, size + 8, size), jnp.float32),
-            pltpu.VMEM((heads, size, size), jnp.float32),
-            pltpu.VMEM((heads, 8, size), jnp.float32),
+            pltpu.VMEM((heads, size + 8, size), f32),
+            pltpu.VMEM((size + 8, size), f32),
+            pltpu.VMEM((n // 2, size + 8, size), f32),
+            pltpu.VMEM((size + 8, size), f32),
+            pltpu.VMEM((size + 8, size), f32),
+            pltpu.VMEM((heads, size, size), f32),
+            pltpu.VMEM((heads, 8, size), f32),
             pltpu.VMEM((heads, 3, size, size), bf),
             pltpu.VMEM((4, chunk, width), bf),
             pltpu.VMEM((2, chunk, width), bf),
             pltpu.VMEM((chunk, width), bf),
             pltpu.VMEM((chunk, width), bf),
             dma,
-            dma((n,)), dma((n,)), dma((n,)), dma((n,)),
-            dma((n, 2)), dma((n, 2)), dma((n, 2)), dma((n, 2)),
-            dma((n,)), dma((n,)), dma((n,)), dma((n,)),
-            dma((n,)), dma((n,)), dma((2,)), dma((2,)), dma, dma,
+            dma((n,)), dma((n,)), dma((n,)), dma((n,)), dma((n,)), dma((n,)),
+            dma((n, 2)), dma((n, 2)), dma((n,)), dma((n,)), dma((n,)), dma((n,)),
+            dma((n // 2,)), dma((n // 2,)), dma((2,)), dma((2,)), dma((2,)), dma((2,)), dma, dma,
         ],
         compiler_params=pltpu.CompilerParams(collective_id=0, has_side_effects=True),
         cost_estimate=pl.CostEstimate(
@@ -529,16 +636,22 @@
     mix = jnp.where(
         rank[:, :, None] == slots[None, None, :], combine[:, :, None], 0.0
     ).reshape(tokens, expert_total * capacity)
-    own_slots = lax.axis_index("tp") * share + jnp.arange(share, dtype=jnp.int32)
+    tp_place = lax.axis_index("tp")
+    fused = lax.axis_size("tp") == 4 and share % 16 == 0 and lax.axis_size("ep") >= 4
+    fused = fused and mixer_in.shape[0] % 512 == 0 and input_gate.shape[0] == 2
+    fused = fused and gate_experts.shape[0] == 1 and is_power(lax.axis_size("ep"))
+    pieces = 2 if fused else 1
+    place = lax.rem(tp_place, 2) * 2 if fused else tp_place
+    own_slots = place * share + jnp.arange(pieces * share, dtype=jnp.int32)
     select = (rank.T[:, None, :] == own_slots[None, :, None]).astype(jnp.bfloat16)
     own_share = (
         jnp.dot(
-            select.reshape(expert_total * share, tokens),
+            select.reshape(expert_total * pieces * share, tokens),
             normed_b,
             preferred_element_type=jnp.float32,
         )
         .astype(jnp.bfloat16)
-        .reshape(expert_total, share, normed_b.shape[1])
+        .reshape(expert_total, pieces * share, normed_b.shape[1])
     )
     normed_a = rms_rows(mixer_in, mixer_gain).astype(jnp.bfloat16)
     prepared = mixer_prepare(
@@ -549,8 +662,7 @@
         head_gain, lax.axis_index("tp") * width_local, width_local
     ).reshape(input_gate.shape[0], -1)
     experts = (own_share, gate_experts[0], up_experts[0], down_experts[0], mix)
-    fused = lax.axis_size("tp") == 4 and share % 16 == 0 and lax.axis_size("ep") > 1
-    if fused and mixer_in.shape[0] % 512 == 0:
+    if fused:
         expert_out, mixer_out = all_fused(*experts, prepared, gain_local, mixer_out_weight)
     else:
         partial = mixer_partial(prepared, gain_local, mixer_out_weight)

time: 119 us -> 120 us (level); the launches traced: 116 us -> 120 us
  Pallas kernels: 90.9 us -> 95.4 us
  matrix products: 11.2 us -> 9.89 us
    pallas_call x1, Pallas kernels: 90.9 us -> 95.4 us  [all_fused(): pl.pallas_call(functools.partial(expert_kernel, (n, share, cap, width, qu...]
    reduce_sum x2, other arithmetic: 2 us -> 3.59 us  [rms_rows(): jnp.mean(widened * widened, axis=-1, keepdims=True) + epsilon]
    dot_general x1, matrix products: 1.71 us -> 0.47 us  [shards(): jnp.dot(normed_b, expert_router, preferred_element_type=jnp.float32)]
    unnamed x28 -> x32, local copies, waits for them, and re-layouts: 4.04 us -> 3.63 us
where the time goes in v1:
time: 120 us
  Pallas kernels  95.4 us (80%)
  matrix products  9.89 us (8%)
  local copies, waits for them, and re-layouts  7.44 us (6%)
  other arithmetic  6.31 us (5%)
    pallas_call x1, Pallas kernels, all_fused(): pl.pallas_call(functools.partial(expert_kernel, (n, share, cap, width, qu...  95.4 us
    dot_general x3, matrix products, project(): jnp.dot(normed_a, weight, preferred_element_type=jnp.float32)  4.75 us
    unnamed x32, local copies, waits for them, and re-layouts  3.63 us
    reduce_sum x2, other arithmetic, rms_rows(): jnp.mean(widened * widened, axis=-1, keepdims=True) + epsilon  3.59 us

profile of v1, /device:TPU:0, one launch (start us, length us, event | category | flops | bytes accessed | tf_op | source)
XLA Modules:
  0.0 120.0 jit_solution(10672971133705828315)
XLA Ops:
  0.6 0.0 copy-start
  0.6 0.0 copy-start.1
  0.7 0.0 copy-start.4
  0.7 0.0 copy-start.6
  0.7 0.0 copy-start.10
  0.7 0.0 copy-start.12
  0.7 1.5 %dynamic-slice_bitcast_fusion.gain_ref = f32[2,128]{1,0:T(2,128)} fusion(f32[1024]{0:T(1024)} %param.24, s32[]{:T(128)S(6)} %select_n.76), kind=kLoop, calls=%fused_computation.86 | loop fusion | bytes 2052 | tf_op jit(solution)/shard_map/reshape | solution.py:663
  2.2 0.1 pad.5.clone
  2.3 1.5 %fusion.3 = f32[256]{0:T(256)S(1)} fusion(bf16[256,2048]{1,0:T(8,128)(2,1)} %param.26), kind=kLoop, calls=%fused_computation.8 | loop fusion | flops 1572608 | bytes 1049600 | tf_op jit(solution)/shard_map/reduce_sum | solution.py:24
  3.8 0.0 copy-start.9
  3.8 2.1 %fusion = f32[512]{0:T(512)S(1)} fusion(bf16[512,2048]{1,0:T(8,128)(2,1)} %param.17), kind=kLoop, calls=%fused_computation.2 | loop fusion | flops 3145216 | bytes 2099200 | tf_op jit(solution)/shard_map/reduce_sum | solution.py:24
  5.9 0.1 eq.139
  6.0 0.0 copy-done.12
  6.0 0.4 fusion.6.cum_ref
  6.4 0.2 slice_reduce_fusion
  6.6 0.0 copy-done.6
  6.7 0.0 copy-done.1
  6.7 0.0 copy-start.11
  6.7 0.5 fusion.43
  7.2 0.5 select_reduce_fusion.1
  7.7 0.0 copy-done.5
  7.7 0.2 fusion.59
  7.9 0.1 subtract_exponential_fusion
  8.0 0.1 copy.25
  8.1 0.1 maximum_maximum_fusion
  8.2 0.1 broadcast_in_dim.94
  8.2 0.2 bitcast_select_fusion.1
  8.5 0.1 bitcast_compare_fusion.1
  8.6 0.1 copy.23
  8.8 0.1 copy.24
  8.9 0.0 copy-start.2
  8.9 0.0 copy-start.7
  9.0 2.5 %convolution_convert_fusion.2.key_ref = bf16[512,256]{1,0:T(8,128)(2,1)S(1)} fusion(bf16[2048,256]{1,0:T(8,128)(2,1)S(1)} %copy-done, bf16[512,2048]{1,0:T(8,128)(2,1)} %param.17, f32[2048]{0:T(1024)S(1)} %copy-done.11, f32[512]{0:T(512)S(1)} %add_rsqrt_fusion), kind=kOutput, calls=%fused_computation.12 | convolution fusion | flops 541196288 | bytes 3418112 | tf_op jit(solution)/shard_map/dot_general | solution.py:500
  11.5 0.0 copy-start.13
  11.5 0.0 copy-start.8
  11.5 0.8 convolution_convert_fusion.3.value_ref
  12.3 0.7 convolution_bitcast_fusion
  13.0 0.7 convolution_bitcast_fusion.1
  13.7 0.7 pad_maximum_fusion.packed_ref
  14.4 1.5 %convolution_convert_fusion.1.query_ref = bf16[512,256]{1,0:T(8,128)(2,1)} fusion(bf16[2048,256]{1,0:T(8,128)(2,1)S(1)} %copy-done.8, bf16[512,2048]{1,0:T(8,128)(2,1)S(1)} %copy-done.2, f32[2048]{0:T(1024)S(1)} %copy-done.11, f32[512]{0:T(512)S(1)} %add_rsqrt_fusion), kind=kOutput, calls=%fused_computation.11 | convolution fusion | flops 541196288 | bytes 3418112 | tf_op jit(solution)/shard_map/dot_general | solution.py:500
  15.8 0.9 copy.26
  16.7 0.3 broadcast_in_dim.90
  17.0 0.3 eq.142
  17.4 1.5 %bitcast_select_fusion.mix_ref = f32[256,1024]{1,0:T(8,128)} fusion(f32[32,8,8,128]{3,2,1,0:T(8,128)S(1)} %bitcast.38, s32[32,8,8,128]{3,2,1,0:T(8,128)S(1)} %bitcast.39, s32[1024]{0:T(1024)S(1)} %iota_bitcast_fusion), kind=kLoop, calls=%fused_computation.17 | loop fusion | flops 524288 | bytes 3149824 | tf_op jit(solution)/shard_map/jit(_where)/select_n | solution.py:636
  18.9 2.2 %convolution_convert_fusion = bf16[512,2048]{1,0:T(8,128)(2,1)} fusion(pred[512,256]{1,0:T(32,128)(4,1)S(1)} %bitcast_compare_fusion.1, bf16[256,2048]{1,0:T(8,128)(2,1)S(1)} %copy-done.1, f32[2048]{0:T(1024)S(1)} %copy-done.4, f32[256]{0:T(256)S(1)} %add_rsqrt_fusion.1), kind=kOutput, calls=%fused_computation.5 | convolution fusion | flops 540016640 | bytes 3286016 | tf_op jit(solution)/shard_map/dot_general | solution.py:648
  21.1 95.4 %shard_map.176 = (bf16[256,512]{1,0:T(8,128)(2,1)}, bf16[128,2048]{1,0:T(8,128)(2,1)}) custom-call(bf16[8,64,2048]{2,1,0:T(8,128)(2,1)} %bitcast.40, bf16[2048,256]{1,0:T(8,128)(2,1)} %bitcast.55, bf16[2048,256]{1,0:T(8,128)(2,1)} %bitcast.56, bf16[256,2048]{1,0:T(8,128)(2,1)} %bitcast.57, f32[256,1024]{1,0:T(8,128)} %bitcast_select_fusion.mix_ref, ...), custom_call_target="tpu_custom_call" | custom-call | flops 60000002048 | bytes 8000000 | tf_op jit(solution)/shard_map/pallas_call | solution.py:435
  116.4 1.9 %copy.37 = bf16[128,2048]{1,0:T(8,128)(2,1)} copy(bf16[128,2048]{1,0:T(8,128)(2,1)} %get-tuple-element.26) | data formatting | bytes 1048576
  118.3 1.7 %copy.38 = bf16[256,512]{1,0:T(8,128)(2,1)} copy(bf16[256,512]{1,0:T(8,128)(2,1)} %get-tuple-element.27) | data formatting | bytes 524288
  (26 shorter events, 0.1 us)
Async XLA Ops:
  0.6 8.3 %copy-start = (bf16[2048,256]{1,0:T(8,128)(2,1)S(1)}, bf16[2048,256]{1,0:T(8,128)(2,1)}, u32[]{:S(2)}) copy-start(bf16[2048,256]{1,0:T(8,128)(2,1)} %param.20) | copy-start | bytes 3145732
  0.6 6.0 %copy-start.1 = (bf16[256,2048]{1,0:T(8,128)(2,1)S(1)}, bf16[256,2048]{1,0:T(8,128)(2,1)}, u32[]{:S(2)}) copy-start(bf16[256,2048]{1,0:T(8,128)(2,1)} %param.26) | copy-start | bytes 3145732
  0.7 6.0 %copy-start.4 = (f32[2048]{0:T(1024)S(1)}, f32[2048]{0:T(1024)}, u32[]{:S(2)}) copy-start(f32[2048]{0:T(1024)} %param.27) | copy-start | bytes 24580
  0.7 6.0 %copy-start.6 = (s32[256,2]{0,1:T(2,128)S(1)}, s32[256,2]{0,1:T(2,128)}, u32[]{:S(2)}) copy-start(s32[256,2]{0,1:T(2,128)} %param.30) | copy-start | bytes 6148
  0.7 6.0 %copy-start.10 = (bf16[2048,2]{0,1:T(2,128)(2,1)S(1)}, bf16[2048,2]{0,1:T(2,128)(2,1)}, u32[]{:S(2)}) copy-start(bf16[2048,2]{0,1:T(2,128)(2,1)} %param.28) | copy-start | bytes 24580
  0.7 5.3 %copy-start.12 = (f32[2,512]{1,0:T(2,128)S(1)}, f32[2,512]{1,0:T(2,128)}, u32[]{:S(2)}) copy-start(f32[2,512]{1,0:T(2,128)} %param.23) | copy-start | bytes 12292
  3.8 3.4 %copy-start.9 = (bf16[2048,8]{0,1:T(8,128)(2,1)S(1)}, bf16[2048,8]{0,1:T(8,128)(2,1)}, u32[]{:S(2)}) copy-start(bf16[2048,8]{0,1:T(8,128)(2,1)} %param.29) | copy-start | bytes 98308
  6.0 1.7 %copy-start.5 = (f32[2,512]{1,0:T(2,128)S(1)}, f32[2,512]{1,0:T(2,128)}, u32[]{:S(2)}) copy-start(f32[2,512]{1,0:T(2,128)} %in_ref.1) | copy-start | bytes 12292
  6.4 9.5 %copy-start.3 = (f32[2,512]{1,0:T(2,128)}, f32[2,512]{1,0:T(2,128)S(1)}, u32[]{:S(2)}) copy-start(f32[2,512]{1,0:T(2,128)S(1)} %fusion.6.cum_ref) | copy-start | bytes 12292
  6.7 2.2 %copy-start.11 = (f32[2048]{0:T(1024)S(1)}, f32[2048]{0:T(1024)}, u32[]{:S(2)}) copy-start(f32[2048]{0:T(1024)} %param.18) | copy-start | bytes 24580
  8.9 2.5 %copy-start.2 = (bf16[512,2048]{1,0:T(8,128)(2,1)S(1)}, bf16[512,2048]{1,0:T(8,128)(2,1)}, u32[]{:S(2)}) copy-start(bf16[512,2048]{1,0:T(8,128)(2,1)} %param.17) | copy-start | bytes 6291460
  8.9 2.5 %copy-start.7 = (bf16[2048,256]{1,0:T(8,128)(2,1)S(1)}, bf16[2048,256]{1,0:T(8,128)(2,1)}, u32[]{:S(2)}) copy-start(bf16[2048,256]{1,0:T(8,128)(2,1)} %param.21) | copy-start | bytes 3145732
  11.5 1.5 %copy-start.13 = (bf16[512,256]{1,0:T(8,128)(2,1)}, bf16[512,256]{1,0:T(8,128)(2,1)S(1)}, u32[]{:S(2)}) copy-start(bf16[512,256]{1,0:T(8,128)(2,1)S(1)} %convolution_convert_fusion.2.key_ref) | copy-start | bytes 786436
  11.5 2.9 %copy-start.8 = (bf16[2048,256]{1,0:T(8,128)(2,1)S(1)}, bf16[2048,256]{1,0:T(8,128)(2,1)}, u32[]{:S(2)}) copy-start(bf16[2048,256]{1,0:T(8,128)(2,1)} %param.19) | copy-start | bytes 3145732
  12.3 3.6 %copy-start.14 = (bf16[512,256]{1,0:T(8,128)(2,1)}, bf16[512,256]{1,0:T(8,128)(2,1)S(1)}, u32[]{:S(2)}) copy-start(bf16[512,256]{1,0:T(8,128)(2,1)S(1)} %convolution_convert_fusion.3.value_ref) | copy-start | bytes 786436

commit v2 on v1

--- a/solution.py
+++ b/solution.py
@@ -31,17 +31,55 @@
     return jnp.exp(moved - peak) * earlier_memory + jnp.exp(later_peak - peak) * later_memory, peak
 
 
-def expert_kernel(
-    sizes, own_ref, gate_ref, up_ref, down_ref, mix_ref,
-    packed_ref, query_ref, key_ref, value_ref, cum_ref, cum_col_ref, in_ref, gain_ref, project_ref,
+def three_parts(matrix):
+    parts = []
+    for _ in range(3):
+        top_part = matrix.astype(jnp.bfloat16)
+        parts.append(top_part)
+        matrix = matrix - top_part.astype(jnp.float32)
+    return parts
+
+
+nn = (((1,), (0,)), ((), ()))
+nt = (((1,), (1,)), ((), ()))
+tn = (((0,), (0,)), ((), ()))
+
+
+def product(left, right, numbers):
+    return lax.dot_general(left, right, numbers, preferred_element_type=jnp.float32)
+
+
+def normalize(source, gain_ref, target):
+    block = 64
+
+    def body(b, carry):
+        place = pl.ds(pl.multiple_of(b * block, block), block)
+        widened = source[place, :].astype(jnp.float32)
+        mean = jnp.mean(widened * widened, axis=-1, keepdims=True)
+        factor = lax.rsqrt(mean + epsilon)
+        target[place, :] = (source[place, :].astype(jnp.float32) * factor * gain_ref[...]).astype(
+            target.dtype
+        )
+        return carry
+
+    lax.fori_loop(0, source.shape[0] // block, body, 0)
+
+
+def whole_kernel(
+    sizes, mixer_hbm, expert_hbm, query_hbm, key_hbm, value_hbm, project_hbm, gate_hbm, up_hbm, down_hbm,
+    mixer_gain_ref, expert_gain_ref, head_gain_ref, in_ref, forget_ref,
+    group_router_ref, expert_router_ref, routes_ref,
     out_ref, mixed_ref,
+    mixer_in, expert_in, query_w, key_w, value_w, project_ref, gate_ref, up_ref, down_ref,
+    normed_a, normed_b, rank, combine, near_rows, far_rows,
+    query_ref, key_ref, value_ref, cum_ref, cum_col_ref, packed_ref, acc,
     rows, part, pin, csum, xin, fin, ret,
     peer, plane, mem, pre, pre_in, state, state_peak, state_parts, mpart, mpin, msum, mxin,
     own_sem, send_a, recv_a, send_x, recv_x, send_p, recv_p,
     send_q, recv_q, send_c, recv_c, send_r, recv_r,
     send_m, recv_m, send_k, recv_k, send_h, recv_h, send_y, recv_y,
 ):
-    n, share, cap, width, quarter = sizes
+    n, share, cap, width, quarter, heads, size = sizes
     near = n // 2
     planes = n // 2
     me, tp = lax.axis_index("ep"), lax.axis_index("tp")
@@ -51,6 +89,10 @@
     pair_cross = lax.rem(pair + 2, 4)
     side, level = lax.rem(me, 2), lax.div(me, 2)
     mate = me + 1 - 2 * side
+    tokens = expert_in.shape[0]
+    length = mixer_in.shape[0]
+    chunk = length // 4
+    scale = size ** (-0.5)
 
     def other(i):
         total, bit = 0, 1
@@ -79,19 +121,31 @@
         )
     pl.semaphore_signal(barrier, inc=1, device_id=(me, pair), device_id_type=MESH)
     pl.semaphore_signal(barrier, inc=1, device_id=(me, cross), device_id_type=MESH)
-    own = pltpu.make_async_copy(own_ref.at[me], rows.at[me, core], own_sem)
-    own.start()
-    pl.semaphore_wait(barrier, n + 1)
+
+    loads = [
+        pltpu.make_async_copy(src, dst, own_sem.at[k])
+        for k, (src, dst) in enumerate(
+            [
+                (expert_hbm, expert_in), (gate_hbm, gate_ref), (up_hbm, up_ref),
+                (down_hbm, down_ref), (mixer_hbm, mixer_in), (key_hbm, key_w),
+                (value_hbm, value_w), (query_hbm, query_w), (project_hbm, project_ref),
+            ]
+        )
+    ]
+    for load in loads:
+        load.start()
 
     def scatter_near(i, place):
-        to = other(i)
-        return remote(own_ref.at[to], rows.at[place, core], send_a.at[i], recv_a.at[i], (to, tp))
+        slot = jnp.maximum(i - 1, 0)
+        return remote(
+            near_rows.at[slot], rows.at[place, core], send_a.at[i], recv_a.at[i], (other(i), tp)
+        )
 
     def scatter_far(i, place):
-        to = other(i)
+        slot = jnp.maximum(i - near, 0)
         mine = pl.ds(pl.multiple_of(column * share, share), share)
         return remote(
-            own_ref.at[to, mine], rows.at[place, core, mine], send_a.at[i], recv_a.at[i], (to, tp)
+            far_rows.at[slot], rows.at[place, core, mine], send_a.at[i], recv_a.at[i], (other(i), tp)
         )
 
     def across(s, which):
@@ -134,15 +188,119 @@
     def mixed_half(k, who):
         return remote(mpart.at[who], mpin.at[k], send_h.at[k], recv_h.at[k], (me, pair))
 
-    def mixed_sum():
-        return remote(msum, mxin, send_y, recv_y, (me, cross))
-
-    heads = packed_ref.shape[0]
-    size = packed_ref.shape[2]
-    length = query_ref.shape[0]
-    chunk = length // 4
-    scale = size ** (-0.5)
+    def mixed_sum(q):
+        return remote(msum.at[q], mxin.at[q], send_y.at[q], recv_y.at[q], (me, cross))
+
     body, top_row, sum_row = slice(0, size), slice(size, size + 1), slice(size + 1, size + 2)
+
+    def picks(e, first, count):
+        slots = lax.broadcasted_iota(jnp.int32, (count, tokens), 0) + first
+        return rank[pl.ds(e, 1), :] == slots.astype(jnp.float32)
+
+    def gathered(parts):
+        select = jnp.concatenate([jnp.where(p, 1.0, 0.0).astype(jnp.bfloat16) for p in parts], axis=0)
+        return product(select, normed_b[...], nn).astype(jnp.bfloat16)
+
+    def prepare_rank():
+        experts = lax.broadcasted_iota(jnp.int32, (n, tokens), 0)
+        matches = (routes_ref[0:1, :] == experts) | (routes_ref[1:2, :] == experts)
+        earlier = lax.broadcasted_iota(jnp.int32, (tokens, tokens), 0)
+        earlier = earlier < lax.broadcasted_iota(jnp.int32, (tokens, tokens), 1)
+        count = product(
+            jnp.where(matches, 1.0, 0.0).astype(jnp.bfloat16),
+            jnp.where(earlier, 1.0, 0.0).astype(jnp.bfloat16),
+            nn,
+        )
+        rank[...] = jnp.where(matches, count, -1.0)
+
+    def prepare_combine():
+        experts = lax.broadcasted_iota(jnp.int32, (n, tokens), 0)
+        groups = group_router_ref.shape[0]
+        expert_logits = product(expert_router_ref[...], normed_b[...], nt)
+        group_logits = product(group_router_ref[...], normed_b[...], nt)
+        group_full = jnp.zeros((n, tokens), jnp.float32)
+        for g in range(groups):
+            inside = (experts >= g * (n // groups)) & (experts < (g + 1) * (n // groups))
+            group_full = group_full + jnp.where(inside, group_logits[g : g + 1, :], 0.0)
+        named = [routes_ref[k : k + 1, :] == experts for k in range(2)]
+        chosen = [jnp.sum(jnp.where(m, expert_logits, 0.0), axis=0, keepdims=True) for m in named]
+        total = jnp.zeros((n, tokens), jnp.float32)
+        for k in range(2):
+            group_pick = jnp.sum(jnp.where(named[k], group_full, 0.0), axis=0, keepdims=True)
+            weight = jax.nn.sigmoid(group_pick) * jax.nn.sigmoid(chosen[k] - chosen[1 - k])
+            total = total + jnp.where(named[k], weight, 0.0)
+        combine[...] = total
+
+    def prepare_near():
+        step_rows = 2 * share
+        moved = gathered([picks(other(i), core * step_rows, step_rows) for i in range(1, near)])
+        for i in range(1, near):
+            near_rows[i - 1] = moved[(i - 1) * step_rows : i * step_rows]
+
+    def prepare_far():
+        first = core * (2 * share) + column * share
+        moved = gathered([picks(other(i), first, share) for i in range(near, n)])
+        for i in range(near, n):
+            far_rows[i - near] = moved[(i - near) * share : (i - near + 1) * share]
+
+    def prepare_own():
+        rows[me] = gathered([picks(me, 0, cap)]).reshape(2, 2 * share, width)
+
+    def ffn(s):
+        x = rows[s].reshape(cap, width)
+        gate_act = jnp.dot(x, gate_ref[...], preferred_element_type=jnp.float32)
+        up_act = jnp.dot(x, up_ref[...], preferred_element_type=jnp.float32)
+        hidden = (gate_act * jax.nn.sigmoid(gate_act) * up_act).astype(jnp.bfloat16)
+        for q in range(4):
+            part[s, q] = jnp.dot(
+                hidden,
+                down_ref[:, q * quarter : (q + 1) * quarter],
+                preferred_element_type=jnp.float32,
+            ).astype(jnp.bfloat16)
+
+    def prepare_gates():
+        log_forget = jnp.minimum(forget_ref[...], 0.0) - jnp.log1p(jnp.exp(-jnp.abs(forget_ref[...])))
+        pieces = jnp.concatenate(
+            [p.astype(jnp.float32) for p in three_parts(log_forget)]
+            + [jnp.zeros((16 - 3 * heads, length), jnp.float32)],
+            axis=0,
+        ).astype(jnp.bfloat16)
+        first = lax.broadcasted_iota(jnp.int32, (length, length), 0)
+        upto = first <= lax.broadcasted_iota(jnp.int32, (length, length), 1)
+        sums = product(pieces, jnp.where(upto, 1.0, 0.0).astype(jnp.bfloat16), nn)
+        cum_ref[...] = sums[2 * heads : 3 * heads] + sums[heads : 2 * heads] + sums[0:heads]
+        back_to = first >= lax.broadcasted_iota(jnp.int32, (length, length), 1)
+        sums = product(jnp.where(back_to, 1.0, 0.0).astype(jnp.bfloat16), pieces, nt)
+        cum_col_ref[...] = (
+            sums[:, 2 * heads : 3 * heads] + sums[:, heads : 2 * heads] + sums[:, 0:heads]
+        )
+
+    def prepare_memory():
+        key_ref[...] = jnp.dot(
+            normed_a[...], key_w[...], preferred_element_type=jnp.float32
+        ).astype(jnp.bfloat16)
+        value_ref[...] = jnp.dot(
+            normed_a[...], value_w[...], preferred_element_type=jnp.float32
+        ).astype(jnp.bfloat16)
+        for h in range(heads):
+            cols = slice(h * size, (h + 1) * size)
+            cum = cum_ref[h : h + 1, :]
+            total = cum_ref[h : h + 1, length - 1 : length]
+            log_weight = total - cum + in_ref[h : h + 1, :]
+            peak = jnp.max(log_weight, axis=1, keepdims=True)
+            weighted = value_ref[:, cols].astype(jnp.float32).T * jnp.exp(log_weight - peak)
+            memory = jnp.zeros((size, size), jnp.float32)
+            for piece in three_parts(weighted)[::-1]:
+                memory = memory + product(piece, key_ref[:, cols], nn)
+            packed_ref[h, body] = memory * scale
+            packed_ref[h, size : size + 8] = jnp.zeros((8, size), jnp.float32)
+            packed_ref[h, top_row] = jnp.broadcast_to(peak, (1, size))
+            packed_ref[h, sum_row] = jnp.broadcast_to(total, (1, size))
+
+    def prepare_query():
+        query_ref[...] = jnp.dot(
+            normed_a[...], query_w[...], preferred_element_type=jnp.float32
+        ).astype(jnp.bfloat16)
 
     def combine_plane():
         to_mate().wait_recv()
@@ -206,17 +364,13 @@
                 state_peak[h, 0:1, :] = peak
 
         for h in range(heads):
-            rest = state[h]
-            for piece in range(3):
-                top_part = rest.astype(jnp.bfloat16)
-                state_parts[h, piece] = top_part
-                rest = rest - top_part.astype(jnp.float32)
+            for piece, value in enumerate(three_parts(state[h])):
+                state_parts[h, piece] = value
 
     def attend(j):
         start = pl.multiple_of(j * chunk, chunk)
         row = start + lax.broadcasted_iota(jnp.int32, (chunk, length), 0)
         causal = row >= lax.broadcasted_iota(jnp.int32, (chunk, length), 1)
-        nt = (((1,), (1,)), ((), ()))
         cell_list = []
         for h in range(heads):
             cols = slice(h * size, (h + 1) * size)
@@ -225,30 +379,35 @@
             within = jnp.where(causal, c - cum_ref[h : h + 1, :] + in_ref[h : h + 1, :], -jnp.inf)
             carried = c + state_peak[h, 0:1, 0:1]
             top = jnp.maximum(jnp.max(within, axis=1, keepdims=True), carried)
-            raw = lax.dot_general(q, key_ref[:, cols], nt, preferred_element_type=jnp.float32)
+            raw = product(q, key_ref[:, cols], nt)
             scores = (raw * scale * jnp.exp(within - top)).astype(jnp.bfloat16)
             cells = jnp.dot(scores, value_ref[:, cols], preferred_element_type=jnp.float32)
             held = jnp.zeros((chunk, size), jnp.float32)
             for piece in (2, 1, 0):
-                held = held + lax.dot_general(
-                    q, state_parts[h, piece], nt, preferred_element_type=jnp.float32
-                )
+                held = held + product(q, state_parts[h, piece], nt)
             cells = cells + jnp.exp(carried - top) * held
             mean = jnp.mean(cells * cells, axis=1, keepdims=True)
-            cell_list.append(
-                (cells * lax.rsqrt(mean + epsilon) * gain_ref[h : h + 1, :]).astype(jnp.bfloat16)
-            )
+            gain = head_gain_ref[pl.ds(tp * heads + h, 1), :]
+            cell_list.append((cells * lax.rsqrt(mean + epsilon) * gain).astype(jnp.bfloat16))
         cell_rows = jnp.concatenate(cell_list, axis=1)
         for q in range(4):
             cols = slice(q * quarter, (q + 1) * quarter)
-            mpart[j, :, cols] = jnp.dot(
+            mpart[j, q] = jnp.dot(
                 cell_rows, project_ref[:, cols], preferred_element_type=jnp.float32
             ).astype(jnp.bfloat16)
 
     begin = 4
 
     def mixer_step(t):
-        @pl.when(t == 2)
+        @pl.when(t == 1)
+        def _():
+            combine_plane()
+
+            @pl.when(inner == 0)
+            def _():
+                send_far()
+
+        @pl.when(t == 3)
         def _():
             combine_levels()
 
@@ -275,28 +434,102 @@
             msum[...] = (
                 mpart[cross].astype(jnp.float32) + mpin[1].astype(jnp.float32)
             ).astype(jnp.bfloat16)
-            mixed_sum().start()
-
-    def first_near(i, carry):
+
+        @pl.when((t >= begin + 2) & (t < begin + 6))
+        def _():
+            mixed_sum(t - begin - 2).start()
+
+    def send_far():
+        def one(t, carry):
+            scatter_far(turn(t), me).start()
+            return carry
+
+        lax.fori_loop(near, n, one, 0)
+
+    def collect(s):
+        halves(s, 1, pair_cross).wait_recv()
+        csum[s] = (
+            part[s, cross].astype(jnp.float32) + pin[s, 1].astype(jnp.float32)
+        ).astype(jnp.bfloat16)
+        summed(s).start()
+
+    def send_halves(s):
+        halves(s, 1, pair_cross).start()
+        halves(s, 0, pair).start()
+
+    prepare_rank()
+    loads[0].wait()
+    normalize(expert_in, expert_gain_ref, normed_b)
+    prepare_near()
+    prepare_far()
+    pl.semaphore_wait(barrier, n + 1)
+    for i in range(1, near):
         scatter_near(i, me).start()
-        return carry
-
-    def first_far(t, carry):
-        scatter_far(turn(t), me).start()
-        return carry
-
+
+    @pl.when(inner == 1)
+    def _():
+        send_far()
+
+    prepare_own()
+    for k in (1, 2, 3):
+        loads[k].wait()
+    ffn(me)
+    send_halves(me)
+    loads[4].wait()
+    normalize(mixer_in, mixer_gain_ref, normed_a)
+    collect(me)
+    prepare_gates()
+    loads[5].wait()
+    loads[6].wait()
+    prepare_memory()
     to_mate().start()
-    lax.fori_loop(1, near - 1, first_near, 0)
-    own.wait()
-    beside(me, core).start()
-    combine_plane()
-    lax.fori_loop(near - 1, near, first_near, 0)
-    lax.fori_loop(near, n, first_far, 0)
+    loads[7].wait()
+    prepare_query()
+    prepare_combine()
+    loads[8].wait()
 
     def step(t, carry):
-        @pl.when(t >= 4)
-        def _():
-            i = turn(t - 4)
+        @pl.when((t >= near + 1) & (t < n + 1))
+        def _():
+            s = other(turn(t - 1))
+            across(s, 1 - column).wait_recv()
+            beside(s, core).start()
+
+        @pl.when(t >= 2)
+        def _():
+            mixer_step(t)
+
+        @pl.when((t >= 2) & (t < n + 1))
+        def _():
+            s = other(turn(t - 1))
+            beside(s, 1 - core).wait_recv()
+            ffn(s)
+            send_halves(s)
+
+        @pl.when(t < near)
+        def _():
+            s = other(t)
+            scatter_near(t, s).wait_recv()
+            beside(s, core).start()
+
+        @pl.when((t >= near) & (t < n))
+        def _():
+            i = turn(t)
+            s = other(i)
+            scatter_far(i, s).wait_recv()
+            across(s, column).start()
+
+        @pl.when(t == 1)
+        def _():
+            mixer_step(t)
+
+        @pl.when((t >= 2) & (t < n + 1))
+        def _():
+            collect(other(turn(t - 1)))
+
+        @pl.when(t >= 2)
+        def _():
+            i = turn(t - 2)
             s = other(i)
             halves(s, 0, pair).wait_recv()
             summed(s).wait_recv()
@@ -315,85 +548,51 @@
             def _():
                 ret[s] = total
 
-        @pl.when((t >= 3) & (t < n + 3))
-        def _():
-            s = other(turn(t - 3))
-            halves(s, 1, pair_cross).wait_recv()
-            csum[s] = (
-                part[s, cross].astype(jnp.float32) + pin[s, 1].astype(jnp.float32)
-            ).astype(jnp.bfloat16)
-            summed(s).start()
-
-        @pl.when((t >= 1) & (t < near))
-        def _():
-            s = other(t)
-            scatter_near(t, s).wait_recv()
-            beside(s, core).start()
-
-        @pl.when((t >= near) & (t < n))
-        def _():
-            i = turn(t)
-            s = other(i)
-            scatter_far(i, s).wait_recv()
-            across(s, column).start()
-
-        @pl.when((t >= near + 1) & (t < n + 1))
-        def _():
-            s = other(turn(t - 1))
-            across(s, 1 - column).wait_recv()
-            beside(s, core).start()
-
-        @pl.when((t >= 2) & (t < n + 2))
-        def _():
-            s = other(turn(t - 2))
-            beside(s, 1 - core).wait_recv()
-            x = rows[s].reshape(cap, width)
-            gate_act = jnp.dot(x, gate_ref[...], preferred_element_type=jnp.float32)
-            up_act = jnp.dot(x, up_ref[...], preferred_element_type=jnp.float32)
-            hidden = (gate_act * jax.nn.sigmoid(gate_act) * up_act).astype(jnp.bfloat16)
-            for q in range(4):
-                part[s, q] = jnp.dot(
-                    hidden,
-                    down_ref[:, q * quarter : (q + 1) * quarter],
-                    preferred_element_type=jnp.float32,
-                ).astype(jnp.bfloat16)
-            halves(s, 1, pair_cross).start()
-            halves(s, 0, pair).start()
-
-        mixer_step(t)
         return carry
 
-    lax.fori_loop(0, n + 4, step, 0)
+    lax.fori_loop(1, n + 2, step, 0)
 
     mixed_half(0, pair).wait_recv()
-    mixed_sum().wait_recv()
-    mixed_ref[...] = (
-        mpart[tp].astype(jnp.float32) + mpin[0].astype(jnp.float32) + mxin[...].astype(jnp.float32)
-    ).astype(mixed_ref.dtype)
-
-    def finish(i, carry):
-        back(i).wait_recv()
+    for q in range(4):
+        mixed_sum(q).wait_recv()
+        cols = slice(q * quarter, (q + 1) * quarter)
+        mixed_ref[:, cols] = (
+            mpart[tp, q].astype(jnp.float32)
+            + mpin[0, q].astype(jnp.float32)
+            + mxin[q].astype(jnp.float32)
+        ).astype(mixed_ref.dtype)
+
+    acc[...] = jnp.zeros_like(acc)
+
+    def finish(t, carry):
+        i = turn(t)
+        s = other(i)
+
+        @pl.when(t > 0)
+        def _():
+            back(i).wait_recv()
+
+        chosen = picks(s, 0, cap)
+        weight = combine[pl.ds(s, 1), :]
+        high_weight = weight.astype(jnp.bfloat16).astype(jnp.float32)
+        table = ret[s]
+        acc[...] += product(
+            jnp.where(chosen, high_weight, 0.0).astype(jnp.bfloat16), table, tn
+        ) + product(jnp.where(chosen, weight - high_weight, 0.0).astype(jnp.bfloat16), table, tn)
         return carry
 
-    lax.fori_loop(1, n, finish, 0)
-    mix = mix_ref[...]
-    high_mix = mix.astype(jnp.bfloat16)
-    low_mix = (mix - high_mix.astype(jnp.float32)).astype(jnp.bfloat16)
-    table = ret[...].reshape(n * cap, quarter)
-    out_ref[...] = (
-        jnp.dot(high_mix, table, preferred_element_type=jnp.float32)
-        + jnp.dot(low_mix, table, preferred_element_type=jnp.float32)
-    ).astype(out_ref.dtype)
+    lax.fori_loop(0, n, finish, 0)
+    out_ref[...] = acc[...].astype(out_ref.dtype)
 
     def drain(i, carry):
         s = other(i)
-        beside(s, core).wait_send()
         halves(s, 0, pair).wait_send()
         halves(s, 1, pair_cross).wait_send()
         summed(s).wait_send()
 
         @pl.when(i > 0)
         def _():
+            beside(s, core).wait_send()
             back(i).wait_send()
 
         @pl.when((i > 0) & (i < near))
@@ -416,31 +615,62 @@
             to_level(d).wait_send()
     mixed_half(0, pair).wait_send()
     mixed_half(1, pair_cross).wait_send()
-    mixed_sum().wait_send()
-
-
-def all_fused(own_share, gate_weight, up_weight, down_weight, mix, prepared, gain, project):
-    n, pieces, width = own_share.shape
-    share = pieces // 2
-    cap = share * 4
+    for q in range(4):
+        mixed_sum(q).wait_send()
+
+
+def all_fused(
+    mixer_in, mixer_gain, query_weight, key_weight, value_weight, input_gate, forget_gate,
+    head_gain, mixer_out_weight, expert_in, expert_gain, group_router, expert_router, routes,
+    gate_weight, up_weight, down_weight,
+):
+    n = expert_router.shape[1]
+    tokens, width = expert_in.shape
+    cap = 4 * tokens // n
+    share = cap // 4
     quarter = width // 4
-    tokens = mix.shape[0]
-    packed, queries, keys, values, cumulative, input_gate = prepared
-    heads, size = packed.shape[0], packed.shape[2]
-    chunk = queries.shape[0] // 4
+    length = mixer_in.shape[0]
+    heads = input_gate.shape[0]
+    inner_width = query_weight.shape[1]
+    size = inner_width // heads
+    hidden = gate_weight.shape[1]
+    chunk = length // 4
     vmem = pl.BlockSpec(memory_space=pltpu.VMEM)
+    whole = pl.BlockSpec(memory_space=pl.ANY)
     dma = pltpu.SemaphoreType.DMA
     bf = jnp.bfloat16
     f32 = jnp.float32
     return pl.pallas_call(
-        functools.partial(expert_kernel, (n, share, cap, width, quarter)),
+        functools.partial(whole_kernel, (n, share, cap, width, quarter, heads, size)),
         out_shape=(
             jax.ShapeDtypeStruct((tokens, quarter), bf),
             jax.ShapeDtypeStruct((chunk, width), bf),
         ),
-        in_specs=[vmem] * 14,
+        in_specs=[whole] * 9 + [vmem] * 8,
         out_specs=(vmem, vmem),
         scratch_shapes=[
+            pltpu.VMEM((length, width), bf),
+            pltpu.VMEM((tokens, width), bf),
+            pltpu.VMEM((width, inner_width), bf),
+            pltpu.VMEM((width, inner_width), bf),
+            pltpu.VMEM((width, inner_width), bf),
+            pltpu.VMEM((inner_width, width), bf),
+            pltpu.VMEM((width, hidden), bf),
+            pltpu.VMEM((width, hidden), bf),
+            pltpu.VMEM((hidden, width), bf),
+            pltpu.VMEM((length, width), bf),
+            pltpu.VMEM((tokens, width), bf),
+            pltpu.VMEM((n, tokens), f32),
+            pltpu.VMEM((n, tokens), f32),
+            pltpu.VMEM((n // 2 - 1, 2 * share, width), bf),
+            pltpu.VMEM((n // 2, share, width), bf),
+            pltpu.VMEM((length, inner_width), bf),
+            pltpu.VMEM((length, inner_width), bf),
+            pltpu.VMEM((length, inner_width), bf),
+            pltpu.VMEM((heads, length), f32),
+            pltpu.VMEM((length, heads), f32),
+            pltpu.VMEM((heads, size + 8, size), f32),
+            pltpu.VMEM((tokens, quarter), f32),
             pltpu.VMEM((n, 2, 2 * share, width), bf),
             pltpu.VMEM((n, 4, cap, quarter), bf),
             pltpu.VMEM((n, 2, cap, quarter), bf),
@@ -456,22 +686,28 @@
             pltpu.VMEM((heads, size, size), f32),
             pltpu.VMEM((heads, 8, size), f32),
             pltpu.VMEM((heads, 3, size, size), bf),
-            pltpu.VMEM((4, chunk, width), bf),
-            pltpu.VMEM((2, chunk, width), bf),
-            pltpu.VMEM((chunk, width), bf),
-            pltpu.VMEM((chunk, width), bf),
-            dma,
+            pltpu.VMEM((4, 4, chunk, quarter), bf),
+            pltpu.VMEM((2, 4, chunk, quarter), bf),
+            pltpu.VMEM((4, chunk, quarter), bf),
+            pltpu.VMEM((4, chunk, quarter), bf),
+            dma((9,)),
             dma((n,)), dma((n,)), dma((n,)), dma((n,)), dma((n,)), dma((n,)),
             dma((n, 2)), dma((n, 2)), dma((n,)), dma((n,)), dma((n,)), dma((n,)),
-            dma((n // 2,)), dma((n // 2,)), dma((2,)), dma((2,)), dma((2,)), dma((2,)), dma, dma,
+            dma((n // 2,)), dma((n // 2,)), dma((2,)), dma((2,)), dma((2,)), dma((2,)),
+            dma((4,)), dma((4,)),
         ],
-        compiler_params=pltpu.CompilerParams(collective_id=0, has_side_effects=True),
+        compiler_params=pltpu.CompilerParams(
+            collective_id=0, has_side_effects=True, vmem_limit_bytes=60 * 1024 * 1024
+        ),
         cost_estimate=pl.CostEstimate(
             flops=60_000_000_000, bytes_accessed=8_000_000, transcendentals=0
         ),
     )(
-        own_share, gate_weight, up_weight, down_weight, mix,
-        packed, queries, keys, values, cumulative, cumulative.T, input_gate, gain, project,
+        mixer_in, expert_in, query_weight, key_weight, value_weight, mixer_out_weight,
+        gate_weight, up_weight, down_weight,
+        mixer_gain.reshape(1, width), expert_gain.reshape(1, width),
+        head_gain.reshape(-1, size), input_gate, forget_gate,
+        group_router.T, expert_router.T, routes.T,
     )
 
 
@@ -608,6 +844,18 @@
     up_experts,
     down_experts,
 ):
+    ranks = lax.axis_size("ep")
+    share = expert_in.shape[0] // expert_router.shape[1]
+    fused = lax.axis_size("tp") == 4 and ranks >= 4 and is_power(ranks) and share % 16 == 0
+    fused = fused and mixer_in.shape[0] % 512 == 0 and input_gate.shape[0] == 2
+    fused = fused and gate_experts.shape[0] == 1
+    if fused:
+        expert_out, mixer_out = all_fused(
+            mixer_in, mixer_gain, query_weight, key_weight, value_weight, input_gate, forget_gate,
+            head_gain, mixer_out_weight, expert_in, expert_gain, group_router, expert_router,
+            routes, gate_experts[0], up_experts[0], down_experts[0],
+        )
+        return (mixer_out, expert_out)
     normed_b = rms_rows(expert_in, expert_gain).astype(jnp.bfloat16)
     tokens = normed_b.shape[0]
     expert_total = expert_router.shape[1]
@@ -636,22 +884,16 @@
     mix = jnp.where(
         rank[:, :, None] == slots[None, None, :], combine[:, :, None], 0.0
     ).reshape(tokens, expert_total * capacity)
-    tp_place = lax.axis_index("tp")
-    fused = lax.axis_size("tp") == 4 and share % 16 == 0 and lax.axis_size("ep") >= 4
-    fused = fused and mixer_in.shape[0] % 512 == 0 and input_gate.shape[0] == 2
-    fused = fused and gate_experts.shape[0] == 1 and is_power(lax.axis_size("ep"))
-    pieces = 2 if fused else 1
-    place = lax.rem(tp_place, 2) * 2 if fused else tp_place
-    own_slots = place * share + jnp.arange(pieces * share, dtype=jnp.int32)
+    own_slots = lax.axis_index("tp") * share + jnp.arange(share, dtype=jnp.int32)
     select = (rank.T[:, None, :] == own_slots[None, :, None]).astype(jnp.bfloat16)
     own_share = (
         jnp.dot(
-            select.reshape(expert_total * pieces * share, tokens),
+            select.reshape(expert_total * share, tokens),
             normed_b,
             preferred_element_type=jnp.float32,
         )
         .astype(jnp.bfloat16)
-        .reshape(expert_total, pieces * share, normed_b.shape[1])
+        .reshape(expert_total, share, normed_b.shape[1])
     )
     normed_a = rms_rows(mixer_in, mixer_gain).astype(jnp.bfloat16)
     prepared = mixer_prepare(
@@ -662,12 +904,9 @@
         head_gain, lax.axis_index("tp") * width_local, width_local
     ).reshape(input_gate.shape[0], -1)
     experts = (own_share, gate_experts[0], up_experts[0], down_experts[0], mix)
-    if fused:
-        expert_out, mixer_out = all_fused(*experts, prepared, gain_local, mixer_out_weight)
-    else:
-        partial = mixer_partial(prepared, gain_local, mixer_out_weight)
-        mixer_out = lax.psum_scatter(partial, "tp", scatter_dimension=0, tiled=True)
-        expert_out = experts_plain(*experts)
+    partial = mixer_partial(prepared, gain_local, mixer_out_weight)
+    mixer_out = lax.psum_scatter(partial, "tp", scatter_dimension=0, tiled=True)
+    expert_out = experts_plain(*experts)
     return (mixer_out, expert_out)
 
 

time: 120 us -> 97.1 us (0.81)
  matrix products: 9.89 us -> 0 us
  other arithmetic: 6.31 us -> 0 us
  local copies, waits for them, and re-layouts: 7.44 us -> 3.55 us
  Pallas kernels: 95.4 us -> 92.6 us
    dot_general x10 -> x0, matrix products: 9.89 us -> none  [the longest x3 4.75 us: project(): jnp.dot(normed_a, weight, preferred_element_type=jnp.float32)]
    reduce_sum x2 -> x0, other arithmetic: 3.59 us -> none  [rms_rows(): jnp.mean(widened * widened, axis=-1, keepdims=True) + epsilon]
    pallas_call x1, Pallas kernels: 95.4 us -> 92.6 us  [all_fused(): pl.pallas_call(functools.partial(whole_kernel, (n, share, cap, width, qua...]
    select_n x3 -> x0, other arithmetic: 1.53 us -> none  [the longest x1 1.49 us: shards(): jnp.where(rank[:, :, None] == slots[None, None, :], combine[:, :, None],...]
    reshape x1 -> x0, local copies, waits for them, and re-layouts: 1.46 us -> none  [shards(): gain_local = lax.dynamic_slice_in_dim(head_gain, lax.axis_index('tp') * w...]
    unnamed x32 -> x2, local copies, waits for them, and re-layouts: 3.63 us -> 3.55 us
where the time goes in v2:
time: 97.1 us; the launch traced here: 96.8 us
  Pallas kernels  92.6 us (95%)
  local copies, waits for them, and re-layouts  3.55 us (4%)
    pallas_call x1, Pallas kernels, all_fused(): pl.pallas_call(functools.partial(whole_kernel, (n, share, cap, width, qua...  92.6 us
    unnamed x2, local copies, waits for them, and re-layouts  3.55 us

profile of v2, /device:TPU:0, one launch (start us, length us, event | category | flops | bytes accessed | tf_op | source)
XLA Modules:
  0.0 96.8 jit_solution(15519203203247790556)
XLA Ops:
  0.6 92.6 %shard_map.176 = (bf16[256,512]{1,0:T(8,128)(2,1)}, bf16[128,2048]{1,0:T(8,128)(2,1)}) custom-call(bf16[512,2048]{1,0:T(8,128)(2,1)} %mixer_hbm.1, bf16[256,2048]{1,0:T(8,128)(2,1)} %expert_hbm.1, bf16[2048,256]{1,0:T(8,128)(2,1)} %query_hbm.1, bf16[2048,256]{1,0:T(8,128)(2,1)} %key_hbm.1, bf16[2048,256]{1,0:T(8,128)(2,1)} %value_hbm.1, ...), custom_call_target="tpu_custom_call" | custom-call | flops 60000002048 | bytes 8000000 | tf_op jit(solution)/shard_map/pallas_call | solution.py:643
  93.3 1.9 %copy.21 = bf16[128,2048]{1,0:T(8,128)(2,1)} copy(bf16[128,2048]{1,0:T(8,128)(2,1)} %get-tuple-element.8) | data formatting | bytes 1048576
  95.1 1.7 %copy.22 = bf16[256,512]{1,0:T(8,128)(2,1)} copy(bf16[256,512]{1,0:T(8,128)(2,1)} %get-tuple-element.9) | data formatting | bytes 524288

commit v3 on v2

--- a/solution.py
+++ b/solution.py
@@ -104,10 +104,25 @@
     high = lax.rem(lax.div(me, near), 2)
     inner = lax.rem(high + lax.div(lax.rem(me, near), near // 2), 2)
 
+    def far_turn(k):
+        half = near // 2
+        return near + half * lax.rem(lax.rem(k, 2) + 1 - inner, 2) + lax.div(k, 2)
+
+    order = [(False, 0), (False, 1), (True, 0), (True, 1)]
+    order += [(False, k) for k in range(2, near - 1)] + [(True, k) for k in range(2, near)]
+    order += [(False, near - 1)] * (near > 2)
+
     def turn(t):
-        half = near // 2
-        swapped = near + lax.rem(t - near + inner * half, near)
-        return jnp.where(t < near, t, swapped)
+        total = 0
+        for place, (far, k) in enumerate(order):
+            total = total + jnp.where(t == place, far_turn(k) if far else k, 0)
+        return total
+
+    def is_far(t):
+        total = t < 0
+        for place, (far, k) in enumerate(order):
+            total = total | (t == place) if far else total
+        return total
 
     def remote(src, dst, send, recv, to):
         return pltpu.make_async_remote_copy(
@@ -170,7 +185,15 @@
         return remote(fin.at[to], ret.at[me], send_r.at[i], recv_r.at[i], (to, tp))
 
     def to_mate():
-        return remote(packed_ref, peer, send_k.at[0], recv_k.at[0], (mate, tp))
+        return remote(
+            packed_ref.at[1 - side], peer.at[1 - side], send_k.at[0], recv_k.at[0], (mate, tp)
+        )
+
+    def from_mate():
+        return remote(packed_ref.at[side], peer.at[side], send_k.at[0], recv_k.at[0], (mate, tp))
+
+    def rest_to_mate():
+        return remote(packed_ref.at[0], peer.at[0], send_k.at[2], recv_k.at[2], (mate, tp))
 
     def to_level(d):
         return remote(
@@ -303,7 +326,7 @@
         ).astype(jnp.bfloat16)
 
     def combine_plane():
-        to_mate().wait_recv()
+        from_mate().wait_recv()
 
         def joined(first, second):
             memory, peak = merged(
@@ -355,6 +378,7 @@
 
         @pl.when(side == 1)
         def _():
+            rest_to_mate().wait_recv()
             for h in range(heads):
                 memory, peak = merged(
                     state[h], state_peak[h, 0:1, :],
@@ -396,18 +420,14 @@
                 cell_rows, project_ref[:, cols], preferred_element_type=jnp.float32
             ).astype(jnp.bfloat16)
 
-    begin = 4
+    begin = n - 1
+
+    def send_far(first):
+        for k in range(first, first + 2):
+            scatter_far(far_turn(k), me).start()
 
     def mixer_step(t):
-        @pl.when(t == 1)
-        def _():
-            combine_plane()
-
-            @pl.when(inner == 0)
-            def _():
-                send_far()
-
-        @pl.when(t == 3)
+        @pl.when(t == begin - 1)
         def _():
             combine_levels()
 
@@ -415,36 +435,36 @@
         def _():
             combine_last()
 
-        @pl.when((t >= begin) & (t < begin + 4))
-        def _():
-            k = t - begin
-            attend(jnp.where(k == 0, pair_cross, jnp.where(k == 1, pair, jnp.where(k == 2, cross, tp))))
-
+            def one(k, carry):
+                later = jnp.where(k == 2, cross, tp)
+                attend(jnp.where(k == 0, pair_cross, jnp.where(k == 1, pair, later)))
+
+                @pl.when(k == 1)
+                def _():
+                    mixed_half(1, pair_cross).start()
+                    mixed_half(0, pair).start()
+
+                return carry
+
+            lax.fori_loop(0, 4, one, 0)
+
+    def mixer_send(t):
         @pl.when(t == begin)
-        def _():
-            mixed_half(1, pair_cross).start()
-
-        @pl.when(t == begin + 1)
-        def _():
-            mixed_half(0, pair).start()
-
-        @pl.when(t == begin + 2)
         def _():
             mixed_half(1, pair_cross).wait_recv()
             msum[...] = (
                 mpart[cross].astype(jnp.float32) + mpin[1].astype(jnp.float32)
             ).astype(jnp.bfloat16)
-
-        @pl.when((t >= begin + 2) & (t < begin + 6))
-        def _():
-            mixed_sum(t - begin - 2).start()
-
-    def send_far():
-        def one(t, carry):
-            scatter_far(turn(t), me).start()
-            return carry
-
-        lax.fori_loop(near, n, one, 0)
+            mixed_sum(0).start()
+
+        @pl.when(t == begin + 1)
+        def _():
+            mixed_sum(1).start()
+
+        @pl.when(t == begin + 2)
+        def _():
+            mixed_sum(2).start()
+            mixed_sum(3).start()
 
     def collect(s):
         halves(s, 1, pair_cross).wait_recv()
@@ -463,12 +483,16 @@
     prepare_near()
     prepare_far()
     pl.semaphore_wait(barrier, n + 1)
-    for i in range(1, near):
-        scatter_near(i, me).start()
+    scatter_near(1, me).start()
+
+    @pl.when(inner == 0)
+    def _():
+        send_far(0)
 
     @pl.when(inner == 1)
     def _():
-        send_far()
+        for i in range(2, near - 1):
+            scatter_near(i, me).start()
 
     prepare_own()
     for k in (1, 2, 3):
@@ -483,53 +507,80 @@
     loads[6].wait()
     prepare_memory()
     to_mate().start()
+
+    @pl.when(inner == 0)
+    def _():
+        for i in range(2, near - 1):
+            scatter_near(i, me).start()
+
+    @pl.when(inner == 1)
+    def _():
+        send_far(0)
+        if near > 2:
+            scatter_near(near - 1, me).start()
+
     loads[7].wait()
     prepare_query()
     prepare_combine()
     loads[8].wait()
 
     def step(t, carry):
-        @pl.when((t >= near + 1) & (t < n + 1))
-        def _():
-            s = other(turn(t - 1))
-            across(s, 1 - column).wait_recv()
-            beside(s, core).start()
-
-        @pl.when(t >= 2)
-        def _():
-            mixer_step(t)
-
-        @pl.when((t >= 2) & (t < n + 1))
-        def _():
-            s = other(turn(t - 1))
+        @pl.when((t >= 3) & (t < n + 2))
+        def _():
+            @pl.when(is_far(t - 2))
+            def _():
+                s = other(turn(t - 2))
+                across(s, 1 - column).wait_recv()
+                beside(s, core).start()
+
+        mixer_step(t)
+
+        @pl.when((t >= 3) & (t < n + 2))
+        def _():
+            s = other(turn(t - 2))
             beside(s, 1 - core).wait_recv()
             ffn(s)
             send_halves(s)
 
-        @pl.when(t < near)
-        def _():
-            s = other(t)
-            scatter_near(t, s).wait_recv()
-            beside(s, core).start()
-
-        @pl.when((t >= near) & (t < n))
+        @pl.when((t >= 3) & (t < n + 2))
+        def _():
+            collect(other(turn(t - 2)))
+
+        mixer_send(t)
+
+        @pl.when(t < n)
         def _():
             i = turn(t)
             s = other(i)
-            scatter_far(i, s).wait_recv()
-            across(s, column).start()
+
+            @pl.when(is_far(t))
+            def _():
+                scatter_far(i, s).wait_recv()
+                across(s, column).start()
+
+            @pl.when(jnp.logical_not(is_far(t)))
+            def _():
+                scatter_near(i, s).wait_recv()
+                beside(s, core).start()
 
         @pl.when(t == 1)
         def _():
-            mixer_step(t)
-
-        @pl.when((t >= 2) & (t < n + 1))
-        def _():
-            collect(other(turn(t - 1)))
-
-        @pl.when(t >= 2)
-        def _():
-            i = turn(t - 2)
+            combine_plane()
+            for first in range(2, near, 2):
+                send_far(first)
+
+            @pl.when(inner == 0)
+            def _():
+                if near > 2:
+                    scatter_near(near - 1, me).start()
+
+            @pl.when(side == 0)
+            def _():
+                rest_to_mate().start()
+
+        @pl.when(t >= 3)
+        def _():
+            i = turn(t - 3)
             s = other(i)
             halves(s, 0, pair).wait_recv()
             summed(s).wait_recv()
@@ -550,7 +601,7 @@
 
         return carry
 
-    lax.fori_loop(1, n + 2, step, 0)
+    lax.fori_loop(1, n + 3, step, 0)
 
     mixed_half(0, pair).wait_recv()
     for q in range(4):
@@ -608,6 +659,11 @@
 
     lax.fori_loop(0, n, drain, 0)
     to_mate().wait_send()
+
+    @pl.when(side == 0)
+    def _():
+        rest_to_mate().wait_send()
+
     prefix_mate().wait_send()
     for d in range(1, planes):
         @pl.when(level + d < planes)
@@ -693,7 +749,7 @@
             dma((9,)),
             dma((n,)), dma((n,)), dma((n,)), dma((n,)), dma((n,)), dma((n,)),
             dma((n, 2)), dma((n, 2)), dma((n,)), dma((n,)), dma((n,)), dma((n,)),
-            dma((n // 2,)), dma((n // 2,)), dma((2,)), dma((2,)), dma((2,)), dma((2,)),
+            dma((n // 2,)), dma((n // 2,)), dma((3,)), dma((3,)), dma((2,)), dma((2,)),
             dma((4,)), dma((4,)),
         ],
         compiler_params=pltpu.CompilerParams(

time: 97.1 us -> 77.9 us (0.80)
  the two profiles are of different devices: /device:TPU:0 before, /device:TPU:21 now
where the time goes in v3:
time: 77.9 us; the launch traced here: 77.6 us
  Pallas kernels  73.4 us (94%)
  local copies, waits for them, and re-layouts  3.55 us (5%)
    pallas_call x1, Pallas kernels, all_fused(): pl.pallas_call(functools.partial(whole_kernel, (n, share, cap, width, qua...  73.4 us
    unnamed x2, local copies, waits for them, and re-layouts  3.55 us

profile of v3, /device:TPU:21, one launch (start us, length us, event | category | flops | bytes accessed | tf_op | source)
XLA Modules:
  0.0 77.6 jit_solution(14552052959567556779)
XLA Ops:
  0.6 73.4 %shard_map.176 = (bf16[256,512]{1,0:T(8,128)(2,1)}, bf16[128,2048]{1,0:T(8,128)(2,1)}) custom-call(bf16[512,2048]{1,0:T(8,128)(2,1)} %mixer_hbm.1, bf16[256,2048]{1,0:T(8,128)(2,1)} %expert_hbm.1, bf16[2048,256]{1,0:T(8,128)(2,1)} %query_hbm.1, bf16[2048,256]{1,0:T(8,128)(2,1)} %key_hbm.1, bf16[2048,256]{1,0:T(8,128)(2,1)} %value_hbm.1, ...), custom_call_target="tpu_custom_call" | custom-call | flops 60000002048 | bytes 8000000 | tf_op jit(solution)/shard_map/pallas_call | solution.py:699
  74.1 1.9 %copy.21 = bf16[128,2048]{1,0:T(8,128)(2,1)} copy(bf16[128,2048]{1,0:T(8,128)(2,1)} %get-tuple-element.8) | data formatting | bytes 1048576
  75.9 1.7 %copy.22 = bf16[256,512]{1,0:T(8,128)(2,1)} copy(bf16[256,512]{1,0:T(8,128)(2,1)} %get-tuple-element.9) | data formatting | bytes 524288

commit v4 on v3

--- a/solution.py
+++ b/solution.py
@@ -426,45 +426,47 @@
         for k in range(first, first + 2):
             scatter_far(far_turn(k), me).start()
 
-    def mixer_step(t):
-        @pl.when(t == begin - 1)
+    def mixer_levels(t):
+        @pl.when(t == begin - 2)
         def _():
             combine_levels()
 
-        @pl.when(t == begin)
+    def mixer_first(t):
+        @pl.when(t == n)
         def _():
             combine_last()
 
             def one(k, carry):
-                later = jnp.where(k == 2, cross, tp)
-                attend(jnp.where(k == 0, pair_cross, jnp.where(k == 1, pair, later)))
-
-                @pl.when(k == 1)
+                attend(jnp.where(k == 0, pair_cross, cross))
+
+                @pl.when(k == 0)
                 def _():
                     mixed_half(1, pair_cross).start()
+
+                return carry
+
+            lax.fori_loop(0, 2, one, 0)
+
+    def mixer_send(t):
+        @pl.when(t == n + 1)
+        def _():
+            mixed_half(1, pair_cross).wait_recv()
+            for q in range(4):
+                msum[q] = (
+                    mpart[cross, q].astype(jnp.float32) + mpin[1, q].astype(jnp.float32)
+                ).astype(jnp.bfloat16)
+                mixed_sum(q).start()
+
+            def one(k, carry):
+                attend(jnp.where(k == 0, pair, tp))
+
+                @pl.when(k == 0)
+                def _():
                     mixed_half(0, pair).start()
 
                 return carry
 
-            lax.fori_loop(0, 4, one, 0)
-
-    def mixer_send(t):
-        @pl.when(t == begin)
-        def _():
-            mixed_half(1, pair_cross).wait_recv()
-            msum[...] = (
-                mpart[cross].astype(jnp.float32) + mpin[1].astype(jnp.float32)
-            ).astype(jnp.bfloat16)
-            mixed_sum(0).start()
-
-        @pl.when(t == begin + 1)
-        def _():
-            mixed_sum(1).start()
-
-        @pl.when(t == begin + 2)
-        def _():
-            mixed_sum(2).start()
-            mixed_sum(3).start()
+            lax.fori_loop(0, 2, one, 0)
 
     def collect(s):
         halves(s, 1, pair_cross).wait_recv()
@@ -524,6 +526,25 @@
     prepare_combine()
     loads[8].wait()
 
+    def finish(t, carry):
+        i = turn(t)
+        s = other(i)
+
+        @pl.when(t > 0)
+        def _():
+            back(i).wait_recv()
+
+        chosen = picks(s, 0, cap)
+        weight = combine[pl.ds(s, 1), :]
+        high_weight = weight.astype(jnp.bfloat16).astype(jnp.float32)
+        table = ret[s]
+        acc[...] += product(
+            jnp.where(chosen, high_weight, 0.0).astype(jnp.bfloat16), table, tn
+        ) + product(jnp.where(chosen, weight - high_weight, 0.0).astype(jnp.bfloat16), table, tn)
+        return carry
+
+    acc[...] = jnp.zeros_like(acc)
+
     def step(t, carry):
         @pl.when((t >= 3) & (t < n + 2))
         def _():
@@ -533,8 +554,6 @@
                 across(s, 1 - column).wait_recv()
                 beside(s, core).start()
 
-        mixer_step(t)
-
         @pl.when((t >= 3) & (t < n + 2))
         def _():
             s = other(turn(t - 2))
@@ -577,6 +596,12 @@
             @pl.when(side == 0)
             def _():
                 rest_to_mate().start()
+
+        mixer_first(t)
+
+        @pl.when(t == n + 2)
+        def _():
+            lax.fori_loop(0, n - 3, finish, 0)
 
         @pl.when(t >= 3)
         def _():
@@ -599,10 +624,13 @@
             def _():
                 ret[s] = total
 
+        mixer_levels(t)
         return carry
 
     lax.fori_loop(1, n + 3, step, 0)
 
+    lax.fori_loop(n - 3, n, finish, 0)
+    out_ref[...] = acc[...].astype(out_ref.dtype)
     mixed_half(0, pair).wait_recv()
     for q in range(4):
         mixed_sum(q).wait_recv()
@@ -613,28 +641,6 @@
             + mxin[q].astype(jnp.float32)
         ).astype(mixed_ref.dtype)
 
-    acc[...] = jnp.zeros_like(acc)
-
-    def finish(t, carry):
-        i = turn(t)
-        s = other(i)
-
-        @pl.when(t > 0)
-        def _():
-            back(i).wait_recv()
-
-        chosen = picks(s, 0, cap)
-        weight = combine[pl.ds(s, 1), :]
-        high_weight = weight.astype(jnp.bfloat16).astype(jnp.float32)
-        table = ret[s]
-        acc[...] += product(
-            jnp.where(chosen, high_weight, 0.0).astype(jnp.bfloat16), table, tn
-        ) + product(jnp.where(chosen, weight - high_weight, 0.0).astype(jnp.bfloat16), table, tn)
-        return carry
-
-    lax.fori_loop(0, n, finish, 0)
-    out_ref[...] = acc[...].astype(out_ref.dtype)
-
     def drain(i, carry):
         s = other(i)
         halves(s, 0, pair).wait_send()
@@ -673,6 +679,11 @@
     mixed_half(1, pair_cross).wait_send()
     for q in range(4):
         mixed_sum(q).wait_send()
+
+
+def hand_over(first_ref, second_ref, first_out, second_out):
+    first_out[...] = first_ref[...]
+    second_out[...] = second_ref[...]
 
 
 def all_fused(
@@ -696,7 +707,7 @@
     dma = pltpu.SemaphoreType.DMA
     bf = jnp.bfloat16
     f32 = jnp.float32
-    return pl.pallas_call(
+    results = pl.pallas_call(
         functools.partial(whole_kernel, (n, share, cap, width, quarter, heads, size)),
         out_shape=(
             jax.ShapeDtypeStruct((tokens, quarter), bf),
@@ -765,6 +776,13 @@
         head_gain.reshape(-1, size), input_gate, forget_gate,
         group_router.T, expert_router.T, routes.T,
     )
+    return pl.pallas_call(
+        hand_over,
+        out_shape=tuple(jax.ShapeDtypeStruct(r.shape, r.dtype) for r in results),
+        in_specs=[vmem, vmem],
+        out_specs=(vmem, vmem),
+        compiler_params=pltpu.CompilerParams(vmem_limit_bytes=60 * 1024 * 1024),
+    )(*results)
 
 
 def experts_plain(own_share, gate_weight, up_weight, down_weight, mix):

time: 77.9 us -> 72.7 us (0.933)
  local copies, waits for them, and re-layouts: 3.55 us -> 0 us
  Pallas kernels: 73.4 us -> 71.8 us
    pallas_call x1, Pallas kernels: 73.4 us -> 69.8 us  [all_fused(): pl.pallas_call(functools.partial(whole_kernel, (n, share, cap, width, qua...]
    unnamed x2 -> x0, local copies, waits for them, and re-layouts: 3.55 us -> none
    pallas_call x0 -> x1, Pallas kernels: none -> 2.02 us  [all_fused(): pl.pallas_call(hand_over, out_shape=tuple((jax.ShapeDtypeStruct(r.shape,...]
where the time goes in v4:
time: 72.7 us; the launch traced here: 72.5 us
  Pallas kernels  71.8 us (99%)
    pallas_call x1, Pallas kernels, all_fused(): pl.pallas_call(functools.partial(whole_kernel, (n, share, cap, width, qua...  69.8 us
    pallas_call x1, Pallas kernels, all_fused(): pl.pallas_call(hand_over, out_shape=tuple((jax.ShapeDtypeStruct(r.shape,...  2.02 us

profile of v4, /device:TPU:21, one launch (start us, length us, event | category | flops | bytes accessed | tf_op | source)
XLA Modules:
  0.0 72.5 jit_solution(4055860950007709909)
XLA Ops:
  0.6 69.8 %shard_map.176 = (bf16[256,512]{1,0:T(8,128)(2,1)}, bf16[128,2048]{1,0:T(8,128)(2,1)}) custom-call(bf16[512,2048]{1,0:T(8,128)(2,1)} %mixer_hbm.1, bf16[256,2048]{1,0:T(8,128)(2,1)} %expert_hbm.1, bf16[2048,256]{1,0:T(8,128)(2,1)} %query_hbm.1, bf16[2048,256]{1,0:T(8,128)(2,1)} %key_hbm.1, bf16[2048,256]{1,0:T(8,128)(2,1)} %value_hbm.1, ...), custom_call_target="tpu_custom_call" | custom-call | flops 60000002048 | bytes 8000000 | tf_op jit(solution)/shard_map/pallas_call | solution.py:710
  70.4 2.0 %shard_map.177 = (bf16[256,512]{1,0:T(8,128)(2,1)}, bf16[128,2048]{1,0:T(8,128)(2,1)}) custom-call(bf16[256,512]{1,0:T(8,128)(2,1)} %get-tuple-element.6.first_ref, bf16[128,2048]{1,0:T(8,128)(2,1)} %get-tuple-element.7.second_ref), custom_call_target="tpu_custom_call" | custom-call | tf_op jit(solution)/shard_map/pallas_call | solution.py:779

commit v5 on v4

--- a/solution.py
+++ b/solution.py
@@ -71,7 +71,7 @@
     group_router_ref, expert_router_ref, routes_ref,
     out_ref, mixed_ref,
     mixer_in, expert_in, query_w, key_w, value_w, project_ref, gate_ref, up_ref, down_ref,
-    normed_a, normed_b, rank, combine, near_rows, far_rows,
+    normed_a, normed_b, rank, rank_in, combine, near_rows, fwd, mine_b, entry_in,
     query_ref, key_ref, value_ref, cum_ref, cum_col_ref, packed_ref, acc,
     rows, part, pin, csum, xin, fin, ret,
     peer, plane, mem, pre, pre_in, state, state_peak, state_parts, mpart, mpin, msum, mxin,
@@ -101,15 +101,11 @@
             bit *= 2
         return total
 
-    high = lax.rem(lax.div(me, near), 2)
-    inner = lax.rem(high + lax.div(lax.rem(me, near), near // 2), 2)
-
     def far_turn(k):
-        half = near // 2
-        return near + half * lax.rem(lax.rem(k, 2) + 1 - inner, 2) + lax.div(k, 2)
-
-    order = [(False, 0), (False, 1), (True, 0), (True, 1)]
-    order += [(False, k) for k in range(2, near - 1)] + [(True, k) for k in range(2, near)]
+        return near + (near // 2) * lax.rem(k, 2) + lax.div(k, 2)
+
+    order = [(False, 0), (False, 1)] + [(False, k) for k in range(2, near - 1)]
+    order += [(True, k) for k in range(near)]
     order += [(False, near - 1)] * (near > 2)
 
     def turn(t):
@@ -156,17 +152,28 @@
             near_rows.at[slot], rows.at[place, core], send_a.at[i], recv_a.at[i], (other(i), tp)
         )
 
-    def scatter_far(i, place):
-        slot = jnp.maximum(i - near, 0)
-        mine = pl.ds(pl.multiple_of(column * share, share), share)
+    def entry():
+        return remote(mine_b, entry_in, send_a.at[0], recv_a.at[0], (other(near), tp))
+
+    def entry_rank():
+        return remote(rank, rank_in, send_a.at[near], recv_a.at[near], (other(near), tp))
+
+    def forward(j):
         return remote(
-            far_rows.at[slot], rows.at[place, core, mine], send_a.at[i], recv_a.at[i], (other(i), tp)
+            fwd.at[j], rows.at[other(near), core, column],
+            send_a.at[near + j], recv_a.at[near + j], (other(j), tp),
+        )
+
+    def arrival(i, s):
+        return remote(
+            fwd.at[i - near], rows.at[s, core, column], send_a.at[i], recv_a.at[i],
+            (other(i - near), tp),
         )
 
     def across(s, which):
-        mine = pl.ds(pl.multiple_of(which * share, share), share)
         return remote(
-            rows.at[s, core, mine], rows.at[s, core, mine], send_x.at[s], recv_x.at[s], (me, cross)
+            rows.at[s, core, which], rows.at[s, core, which],
+            send_x.at[s], recv_x.at[s], (me, cross),
         )
 
     def beside(s, which):
@@ -216,13 +223,17 @@
 
     body, top_row, sum_row = slice(0, size), slice(size, size + 1), slice(size + 1, size + 2)
 
-    def picks(e, first, count):
-        slots = lax.broadcasted_iota(jnp.int32, (count, tokens), 0) + first
-        return rank[pl.ds(e, 1), :] == slots.astype(jnp.float32)
-
-    def gathered(parts):
-        select = jnp.concatenate([jnp.where(p, 1.0, 0.0).astype(jnp.bfloat16) for p in parts], axis=0)
-        return product(select, normed_b[...], nn).astype(jnp.bfloat16)
+    def picks(table, e):
+        slots = lax.broadcasted_iota(jnp.int32, (cap, tokens), 0)
+        return table[pl.ds(e, 1), :] == slots.astype(jnp.float32)
+
+    def selection(table, experts):
+        return jnp.concatenate(
+            [jnp.where(picks(table, e), 1.0, 0.0).astype(jnp.bfloat16) for e in experts], axis=0
+        )
+
+    def features(q):
+        return pl.ds(pl.multiple_of(q * quarter, quarter), quarter)
 
     def prepare_rank():
         experts = lax.broadcasted_iota(jnp.int32, (n, tokens), 0)
@@ -255,22 +266,30 @@
         combine[...] = total
 
     def prepare_near():
-        step_rows = 2 * share
-        moved = gathered([picks(other(i), core * step_rows, step_rows) for i in range(1, near)])
-        for i in range(1, near):
-            near_rows[i - 1] = moved[(i - 1) * step_rows : i * step_rows]
-
-    def prepare_far():
-        first = core * (2 * share) + column * share
-        moved = gathered([picks(other(i), first, share) for i in range(near, n)])
-        for i in range(near, n):
-            far_rows[i - near] = moved[(i - near) * share : (i - near + 1) * share]
+        select = selection(rank, [other(i) for i in range(1, near)])
+        for c in range(2):
+            moved = product(select, normed_b[:, features(2 * c + core)], nn).astype(jnp.bfloat16)
+            for i in range(1, near):
+                near_rows[i - 1, c] = moved[(i - 1) * cap : i * cap]
 
     def prepare_own():
-        rows[me] = gathered([picks(me, 0, cap)]).reshape(2, 2 * share, width)
+        moved = product(selection(rank, [me]), normed_b[...], nn).astype(jnp.bfloat16)
+        for q in range(4):
+            rows[me, q % 2, q // 2] = moved[:, q * quarter : (q + 1) * quarter]
+
+    def redistribute():
+        entry_rank().wait_recv()
+        entry().wait_recv()
+        select = selection(rank_in, [other(j) for j in range(near)])
+        moved = product(select, entry_in[...], nn).astype(jnp.bfloat16)
+        for j in range(1, near):
+            fwd[j] = moved[j * cap : (j + 1) * cap]
+        rows[other(near), core, column] = moved[0:cap]
+        for j in range(1, near):
+            forward(j).start()
 
     def ffn(s):
-        x = rows[s].reshape(cap, width)
+        x = jnp.concatenate([rows[s, q % 2, q // 2] for q in range(4)], axis=1)
         gate_act = jnp.dot(x, gate_ref[...], preferred_element_type=jnp.float32)
         up_act = jnp.dot(x, up_ref[...], preferred_element_type=jnp.float32)
         hidden = (gate_act * jax.nn.sigmoid(gate_act) * up_act).astype(jnp.bfloat16)
@@ -422,12 +441,8 @@
 
     begin = n - 1
 
-    def send_far(first):
-        for k in range(first, first + 2):
-            scatter_far(far_turn(k), me).start()
-
     def mixer_levels(t):
-        @pl.when(t == begin - 2)
+        @pl.when(t == 4)
         def _():
             combine_levels()
 
@@ -455,6 +470,12 @@
                 msum[q] = (
                     mpart[cross, q].astype(jnp.float32) + mpin[1, q].astype(jnp.float32)
                 ).astype(jnp.bfloat16)
+            for q in range(0):
+                mixed_sum(q).start()
+
+        @pl.when(t == n + 1)
+        def _():
+            for q in range(0, 4):
                 mixed_sum(q).start()
 
             def one(k, carry):
@@ -482,25 +503,19 @@
     prepare_rank()
     loads[0].wait()
     normalize(expert_in, expert_gain_ref, normed_b)
+    mine_b[...] = normed_b[:, features(tp)]
     prepare_near()
-    prepare_far()
     pl.semaphore_wait(barrier, n + 1)
+    entry_rank().start()
+    entry().start()
     scatter_near(1, me).start()
-
-    @pl.when(inner == 0)
-    def _():
-        send_far(0)
-
-    @pl.when(inner == 1)
-    def _():
-        for i in range(2, near - 1):
-            scatter_near(i, me).start()
-
     prepare_own()
     for k in (1, 2, 3):
         loads[k].wait()
     ffn(me)
     send_halves(me)
+    for i in range(2, near - 1):
+        scatter_near(i, me).start()
     loads[4].wait()
     normalize(mixer_in, mixer_gain_ref, normed_a)
     collect(me)
@@ -509,18 +524,6 @@
     loads[6].wait()
     prepare_memory()
     to_mate().start()
-
-    @pl.when(inner == 0)
-    def _():
-        for i in range(2, near - 1):
-            scatter_near(i, me).start()
-
-    @pl.when(inner == 1)
-    def _():
-        send_far(0)
-        if near > 2:
-            scatter_near(near - 1, me).start()
-
     loads[7].wait()
     prepare_query()
     prepare_combine()
@@ -534,7 +537,7 @@
         def _():
             back(i).wait_recv()
 
-        chosen = picks(s, 0, cap)
+        chosen = picks(rank, s)
         weight = combine[pl.ds(s, 1), :]
         high_weight = weight.astype(jnp.bfloat16).astype(jnp.float32)
         table = ret[s]
@@ -546,52 +549,65 @@
     acc[...] = jnp.zeros_like(acc)
 
     def step(t, carry):
-        @pl.when((t >= 3) & (t < n + 2))
-        def _():
-            @pl.when(is_far(t - 2))
+        working = (t == 2) | ((t > 3) & (t < n + 2))
+        now = jnp.where(t == 2, 1, t - 2)
+
+        @pl.when(working)
+        def _():
+            @pl.when(is_far(now))
             def _():
-                s = other(turn(t - 2))
+                s = other(turn(now))
                 across(s, 1 - column).wait_recv()
                 beside(s, core).start()
 
-        @pl.when((t >= 3) & (t < n + 2))
-        def _():
-            s = other(turn(t - 2))
+        @pl.when(working)
+        def _():
+            s = other(turn(now))
             beside(s, 1 - core).wait_recv()
             ffn(s)
             send_halves(s)
 
-        @pl.when((t >= 3) & (t < n + 2))
-        def _():
-            collect(other(turn(t - 2)))
+        @pl.when(working)
+        def _():
+            collect(other(turn(now)))
 
         mixer_send(t)
 
-        @pl.when(t < n)
-        def _():
-            i = turn(t)
+        @pl.when(t == 2)
+        def _():
+            redistribute()
+
+        @pl.when(t == 4)
+        def _():
+            if near > 2:
+                scatter_near(near - 1, me).start()
+
+        def arrive(place, carry):
+            i = turn(place)
             s = other(i)
 
-            @pl.when(is_far(t))
+            @pl.when(is_far(place))
             def _():
-                scatter_far(i, s).wait_recv()
+                @pl.when(i > near)
+                def _():
+                    arrival(i, s).wait_recv()
+
                 across(s, column).start()
 
-            @pl.when(jnp.logical_not(is_far(t)))
+            @pl.when(jnp.logical_not(is_far(place)))
             def _():
                 scatter_near(i, s).wait_recv()
                 beside(s, core).start()
 
+            return carry
+
+        begins = jnp.where(t > near + 1, jnp.where(t == n - 1, n - 1, n), t)
+        ends = jnp.where(t == near + 1, t + 2, t + 1)
+        lax.fori_loop(jnp.minimum(begins, n), jnp.minimum(ends, n), arrive, 0)
+
         @pl.when(t == 1)
         def _():
             combine_plane()
-            for first in range(2, near, 2):
-                send_far(first)
-
-            @pl.when(inner == 0)
-            def _():
-                if near > 2:
-                    scatter_near(near - 1, me).start()
 
             @pl.when(side == 0)
             def _():
@@ -658,12 +674,16 @@
 
         @pl.when(i >= near)
         def _():
-            scatter_far(i, me).wait_send()
             across(s, column).wait_send()
+            @pl.when(i > near)
+            def _():
+                forward(i - near).wait_send()
 
         return carry
 
     lax.fori_loop(0, n, drain, 0)
+    entry().wait_send()
+    entry_rank().wait_send()
     to_mate().wait_send()
 
     @pl.when(side == 0)
@@ -729,8 +749,11 @@
             pltpu.VMEM((tokens, width), bf),
             pltpu.VMEM((n, tokens), f32),
             pltpu.VMEM((n, tokens), f32),
-            pltpu.VMEM((n // 2 - 1, 2 * share, width), bf),
-            pltpu.VMEM((n // 2, share, width), bf),
+            pltpu.VMEM((n, tokens), f32),
+            pltpu.VMEM((n // 2 - 1, 2, cap, quarter), bf),
+            pltpu.VMEM((n // 2, cap, quarter), bf),
+            pltpu.VMEM((tokens, quarter), bf),
+            pltpu.VMEM((tokens, quarter), bf),
             pltpu.VMEM((length, inner_width), bf),
             pltpu.VMEM((length, inner_width), bf),
             pltpu.VMEM((length, inner_width), bf),
@@ -738,7 +761,7 @@
             pltpu.VMEM((length, heads), f32),
             pltpu.VMEM((heads, size + 8, size), f32),
             pltpu.VMEM((tokens, quarter), f32),
-            pltpu.VMEM((n, 2, 2 * share, width), bf),
+            pltpu.VMEM((n, 2, 2, cap, quarter), bf),
             pltpu.VMEM((n, 4, cap, quarter), bf),
             pltpu.VMEM((n, 2, cap, quarter), bf),
             pltpu.VMEM((n, cap, quarter), bf),

time: 72.7 us -> 70.2 us (0.966)
  the two profiles are of different devices: /device:TPU:21 before, /device:TPU:0 now
where the time goes in v5:
time: 70.2 us; the launch traced here: 69.2 us
  Pallas kernels  68.6 us (98%)
    pallas_call x1, Pallas kernels, all_fused(): pl.pallas_call(functools.partial(whole_kernel, (n, share, cap, width, qua...  66.5 us
    pallas_call x1, Pallas kernels, all_fused(): pl.pallas_call(hand_over, out_shape=tuple((jax.ShapeDtypeStruct(r.shape,...  2.02 us

profile of v5, /device:TPU:0, one launch (start us, length us, event | category | flops | bytes accessed | tf_op | source)
XLA Modules:
  0.0 69.2 jit_solution(2165933946030533091)
XLA Ops:
  0.6 66.5 %shard_map.176 = (bf16[256,512]{1,0:T(8,128)(2,1)}, bf16[128,2048]{1,0:T(8,128)(2,1)}) custom-call(bf16[512,2048]{1,0:T(8,128)(2,1)} %mixer_hbm.1, bf16[256,2048]{1,0:T(8,128)(2,1)} %expert_hbm.1, bf16[2048,256]{1,0:T(8,128)(2,1)} %query_hbm.1, bf16[2048,256]{1,0:T(8,128)(2,1)} %key_hbm.1, bf16[2048,256]{1,0:T(8,128)(2,1)} %value_hbm.1, ...), custom_call_target="tpu_custom_call" | custom-call | flops 60000002048 | bytes 8000000 | tf_op jit(solution)/shard_map/pallas_call | solution.py:730
  67.2 2.0 %shard_map.177 = (bf16[256,512]{1,0:T(8,128)(2,1)}, bf16[128,2048]{1,0:T(8,128)(2,1)}) custom-call(bf16[256,512]{1,0:T(8,128)(2,1)} %get-tuple-element.6.first_ref, bf16[128,2048]{1,0:T(8,128)(2,1)} %get-tuple-element.7.second_ref), custom_call_target="tpu_custom_call" | custom-call | tf_op jit(solution)/shard_map/pallas_call | solution.py:802

commit v6 on v5

--- a/solution.py
+++ b/solution.py
@@ -447,7 +447,7 @@
             combine_levels()
 
     def mixer_first(t):
-        @pl.when(t == n)
+        @pl.when(t == n + 1)
         def _():
             combine_last()
 
@@ -461,23 +461,17 @@
                 return carry
 
             lax.fori_loop(0, 2, one, 0)
-
-    def mixer_send(t):
-        @pl.when(t == n + 1)
-        def _():
             mixed_half(1, pair_cross).wait_recv()
             for q in range(4):
                 msum[q] = (
                     mpart[cross, q].astype(jnp.float32) + mpin[1, q].astype(jnp.float32)
                 ).astype(jnp.bfloat16)
-            for q in range(0):
+            for q in range(4):
                 mixed_sum(q).start()
 
-        @pl.when(t == n + 1)
-        def _():
-            for q in range(0, 4):
-                mixed_sum(q).start()
-
+    def mixer_late(t):
+        @pl.when(t == n + 2)
+        def _():
             def one(k, carry):
                 attend(jnp.where(k == 0, pair, tp))
 
@@ -548,17 +542,19 @@
 
     acc[...] = jnp.zeros_like(acc)
 
+    collects = {2: (1, 2), n + 1: (n - 2, n)}
+    late_collects = {n - 1: (n - 3, n - 2)}
+    collects.update({t: (t - 2, t - 1) for t in range(4, n - 1)})
+    delivers = {n + 1: (n - 3, n - 2), n + 2: (n - 2, n - 1), n + 3: (n - 1, n)}
+    delivers.update({t: (t - 3, t - 2) for t in range(3, n)})
+
+    def span(table, t):
+        low = sum(jnp.where(t == k, v[0], 0) for k, v in sorted(table.items()))
+        return low, sum(jnp.where(t == k, v[1], 0) for k, v in sorted(table.items()))
+
     def step(t, carry):
         working = (t == 2) | ((t > 3) & (t < n + 2))
         now = jnp.where(t == 2, 1, t - 2)
-
-        @pl.when(working)
-        def _():
-            @pl.when(is_far(now))
-            def _():
-                s = other(turn(now))
-                across(s, 1 - column).wait_recv()
-                beside(s, core).start()
 
         @pl.when(working)
         def _():
@@ -567,11 +563,11 @@
             ffn(s)
             send_halves(s)
 
-        @pl.when(working)
-        def _():
-            collect(other(turn(now)))
-
-        mixer_send(t)
+        def gather(place, carry):
+            collect(other(turn(place)))
+            return carry
+
+        lax.fori_loop(*span(collects, t), gather, 0)
 
         @pl.when(t == 2)
         def _():
@@ -613,15 +609,21 @@
             def _():
                 rest_to_mate().start()
 
+        @pl.when(is_far(t - 1))
+        def _():
+            s = other(turn(t - 1))
+            across(s, 1 - column).wait_recv()
+            beside(s, core).start()
+
+        lax.fori_loop(*span(late_collects, t), gather, 0)
         mixer_first(t)
 
-        @pl.when(t == n + 2)
+        @pl.when(t == n + 3)
         def _():
             lax.fori_loop(0, n - 3, finish, 0)
 
-        @pl.when(t >= 3)
-        def _():
-            i = turn(t - 3)
+        def deliver(place, carry):
+            i = turn(place)
             s = other(i)
             halves(s, 0, pair).wait_recv()
             summed(s).wait_recv()
@@ -640,10 +642,14 @@
             def _():
                 ret[s] = total
 
+            return carry
+
+        lax.fori_loop(*span(delivers, t), deliver, 0)
         mixer_levels(t)
+        mixer_late(t)
         return carry
 
-    lax.fori_loop(1, n + 3, step, 0)
+    lax.fori_loop(1, n + 4, step, 0)
 
     lax.fori_loop(n - 3, n, finish, 0)
     out_ref[...] = acc[...].astype(out_ref.dtype)

time: 70.2 us -> 68.2 us (0.972)
  Pallas kernels: 68.6 us -> 67.3 us
    pallas_call x1, Pallas kernels: 66.5 us -> 65.2 us  [all_fused(): pl.pallas_call(functools.partial(whole_kernel, (n, share, cap, width, qua...]
where the time goes in v6:
time: 68.2 us; the launch traced here: 67.9 us
  Pallas kernels  67.3 us (99%)
    pallas_call x1, Pallas kernels, all_fused(): pl.pallas_call(functools.partial(whole_kernel, (n, share, cap, width, qua...  65.2 us
    pallas_call x1, Pallas kernels, all_fused(): pl.pallas_call(hand_over, out_shape=tuple((jax.ShapeDtypeStruct(r.shape,...  2.02 us

profile of v6, /device:TPU:0, one launch (start us, length us, event | category | flops | bytes accessed | tf_op | source)
XLA Modules:
  0.0 67.9 jit_solution(3088023556515392501)
XLA Ops:
  0.6 65.2 %shard_map.176 = (bf16[256,512]{1,0:T(8,128)(2,1)}, bf16[128,2048]{1,0:T(8,128)(2,1)}) custom-call(bf16[512,2048]{1,0:T(8,128)(2,1)} %mixer_hbm.1, bf16[256,2048]{1,0:T(8,128)(2,1)} %expert_hbm.1, bf16[2048,256]{1,0:T(8,128)(2,1)} %query_hbm.1, bf16[2048,256]{1,0:T(8,128)(2,1)} %key_hbm.1, bf16[2048,256]{1,0:T(8,128)(2,1)} %value_hbm.1, ...), custom_call_target="tpu_custom_call" | custom-call | flops 60000002048 | bytes 8000000 | tf_op jit(solution)/shard_map/pallas_call | solution.py:736
  65.9 2.0 %shard_map.177 = (bf16[256,512]{1,0:T(8,128)(2,1)}, bf16[128,2048]{1,0:T(8,128)(2,1)}) custom-call(bf16[256,512]{1,0:T(8,128)(2,1)} %get-tuple-element.6.first_ref, bf16[128,2048]{1,0:T(8,128)(2,1)} %get-tuple-element.7.second_ref), custom_call_target="tpu_custom_call" | custom-call | tf_op jit(solution)/shard_map/pallas_call | solution.py:808

commit v7 on v6

--- a/solution.py
+++ b/solution.py
@@ -143,8 +143,7 @@
             ]
         )
     ]
-    for load in loads:
-        load.start()
+    loads[0].start()
 
     def scatter_near(i, place):
         slot = jnp.maximum(i - 1, 0)
@@ -496,6 +495,8 @@
 
     prepare_rank()
     loads[0].wait()
+    for load in loads[1:]:
+        load.start()
     normalize(expert_in, expert_gain_ref, normed_b)
     mine_b[...] = normed_b[:, features(tp)]
     prepare_near()
@@ -707,9 +708,27 @@
         mixed_sum(q).wait_send()
 
 
-def hand_over(first_ref, second_ref, first_out, second_out):
-    first_out[...] = first_ref[...]
-    second_out[...] = second_ref[...]
+def hand_over(first_ref, second_ref, first_out, second_out, first_held, second_held, taken, given):
+    moves = []
+    for source, held, target in (
+        (second_ref, second_held, second_out), (first_ref, first_held, first_out)
+    ):
+        half = source.shape[0] // 2
+        for k in range(2):
+            part, place = pl.ds(k * half, half), len(moves)
+            moves.append(
+                (
+                    pltpu.make_async_copy(source.at[part], held.at[part], taken.at[place]),
+                    pltpu.make_async_copy(held.at[part], target.at[part], given.at[place]),
+                )
+            )
+    for take, _ in moves:
+        take.start()
+    for take, give in moves:
+        take.wait()
+        give.start()
+    for _, give in moves:
+        give.wait()
 
 
 def all_fused(
@@ -808,8 +827,9 @@
     return pl.pallas_call(
         hand_over,
         out_shape=tuple(jax.ShapeDtypeStruct(r.shape, r.dtype) for r in results),
-        in_specs=[vmem, vmem],
-        out_specs=(vmem, vmem),
+        in_specs=[whole, whole],
+        out_specs=(whole, whole),
+        scratch_shapes=[pltpu.VMEM(r.shape, r.dtype) for r in results] + [dma((4,)), dma((4,))],
         compiler_params=pltpu.CompilerParams(vmem_limit_bytes=60 * 1024 * 1024),
     )(*results)
 

time: 68.2 us -> 68.1 us (level)
  no operation moved by 1% of the time
where the time goes in v7:
time: 68.1 us; the launch traced here: 67.8 us
  Pallas kernels  67.1 us (99%)
    pallas_call x1, Pallas kernels, all_fused(): pl.pallas_call(functools.partial(whole_kernel, (n, share, cap, width, qua...  65.2 us
    pallas_call x1, Pallas kernels, all_fused(): pl.pallas_call(hand_over, out_shape=tuple((jax.ShapeDtypeStruct(r.shape,...  1.89 us

profile of v7, /device:TPU:0, one launch (start us, length us, event | category | flops | bytes accessed | tf_op | source)
XLA Modules:
  0.0 67.8 jit_solution(12695897600479077750)
XLA Ops:
  0.6 65.2 %shard_map.176 = (bf16[256,512]{1,0:T(8,128)(2,1)}, bf16[128,2048]{1,0:T(8,128)(2,1)}) custom-call(bf16[512,2048]{1,0:T(8,128)(2,1)} %mixer_hbm.1, bf16[256,2048]{1,0:T(8,128)(2,1)} %expert_hbm.1, bf16[2048,256]{1,0:T(8,128)(2,1)} %query_hbm.1, bf16[2048,256]{1,0:T(8,128)(2,1)} %key_hbm.1, bf16[2048,256]{1,0:T(8,128)(2,1)} %value_hbm.1, ...), custom_call_target="tpu_custom_call" | custom-call | flops 60000002048 | bytes 8000000 | tf_op jit(solution)/shard_map/pallas_call | solution.py:755
  65.9 1.9 %shard_map.177 = (bf16[256,512]{1,0:T(8,128)(2,1)}, bf16[128,2048]{1,0:T(8,128)(2,1)}) custom-call(bf16[256,512]{1,0:T(8,128)(2,1)} %get-tuple-element.6.first_ref, bf16[128,2048]{1,0:T(8,128)(2,1)} %get-tuple-element.7.second_ref), custom_call_target="tpu_custom_call" | custom-call | tf_op jit(solution)/shard_map/pallas_call | solution.py:827
